TPU v7x, 256 devices: a whole 4x4x8 slice. The times are simulated.
256 devices in a mesh: sp: 16 (over y, x), tp: 16 (over z, core).
Axes of the slice: x: 4, y: 4, z: 8, core: 2. Of those that a mesh axis runs over, the one named last changes fastest.
Arguments:
- upstream: bfloat16 [4096, 4096], P('sp', 'tp'), may hold values from -6 to 6
- stream: bfloat16 [4096, 4096], P('sp', 'tp'), may hold values from -400 to 400
- norm_gain: float32 [4096], P('tp'), may hold values from 0.1 to 1.9
- routes: int32 [4096, 2], P('sp'), may hold values from 0 to 15, all different within a row; in each aligned block of 256 rows (0 to 255, 256 to 511, ...) at most 48 rows name the same one
- route_weights: float32 [4096, 2], P('sp'), may hold values from 0.1 to 1
- w_gate: bfloat16 [16, 4096, 2048], P('sp', None, 'tp'), may hold values from -0.09375 to 0.09375
- w_up: bfloat16 [16, 4096, 2048], P('sp', None, 'tp'), may hold values from -0.09375 to 0.09375
- w_down: bfloat16 [16, 2048, 4096], P('sp', 'tp'), may hold values from -0.125 to 0.125
- value_in: bfloat16 [4096, 2048], P('sp', 'tp'), may hold values from -6 to 6
- gate_in: bfloat16 [4096, 2048], P('sp', 'tp'), may hold values from -6 to 6
- conv_pre: bfloat16 [4096, 2048], P('sp', 'tp'), may hold values from -200 to 200
- ln_gain: float32 [2048], P('tp'), may hold values from 0.1 to 1.9
- conv_taps: float32 [31, 2048], P(None, 'tp'), may hold values from -1 to 1
- w_out: bfloat16 [2048, 4096], P('tp'), may hold values from -0.125 to 0.125
Outputs:
- grad_gate: float32 [16, 4096, 2048], P('sp', None, 'tp')
- grad_up: float32 [16, 4096, 2048], P('sp', None, 'tp')
- grad_down: float32 [16, 2048, 4096], P('sp', 'tp')
- grad_out: float32 [2048, 4096], P('tp', 'sp')
- value_grad: bfloat16 [4096, 2048], P('sp', 'tp')
- gate_grad: bfloat16 [4096, 2048], P('sp', 'tp')
Inputs may be any that keep to these rules, and one draw needn't show every extreme that they name: `routes`: each token names two different experts. Among the tokens of one index of sp no expert is named more than 48 times, and in every draw some expert exactly 48 times.
All inputs are finite; a program needn't handle non-finite values.
Results may differ from a plain program's by a relative error of at most 0.0071.
Values may be sent and summed in bfloat16 or wider, within the bound.
No kernel may reach another device: no remote copies, remote signals or barrier semaphores. Data moves between devices by JAX's collectives and lax.ppermute only.
A program may use at most 128 MiB of HBM per device.

v0:
```python
import jax
import jax.numpy as jnp
from jax import lax
from jax.experimental import pallas as pl
from jax.experimental.pallas import tpu as pltpu
from jax.sharding import Mesh, PartitionSpec as P

EPSILON = 1e-06
TP = ("z", "c")
BF = jnp.bfloat16
F4 = jnp.float32


def of_everyone(value):
    count = 16
    everything = lax.all_to_all(
        jnp.broadcast_to(value[None], (count, *value.shape)), TP, 0, 0, tiled=True
    )
    return jnp.sum(everything, axis=0)


def in_one(arrays):
    total = of_everyone(jnp.concatenate([a.reshape(-1) for a in arrays]))
    out, at = [], 0
    for a in arrays:
        out.append(total[at : at + a.size].reshape(a.shape))
        at += a.size
    return out


def right(x):
    n = lax.axis_size("z")
    return lax.ppermute(x, "z", [(i, (i + 1) % n) for i in range(n)])


def left(x):
    n = lax.axis_size("z")
    return lax.ppermute(x, "z", [(i, (i - 1) % n) for i in range(n)])


def hops(x, n_hops):
    n = lax.axis_size("z")
    return lax.ppermute(x, "z", [(i, (i + n_hops) % n) for i in range(n)])


def swap(x):
    return lax.ppermute(x, "c", [(0, 1), (1, 0)])


def silu_slope(values):
    logistic = jax.nn.sigmoid(values)
    return logistic * (1.0 + values * (1.0 - logistic))


def dot(a, b, ca, cb):
    return lax.dot_general(a, b, (((ca,), (cb,)), ((), ())), preferred_element_type=F4)


VMEM = pl.BlockSpec(memory_space=pltpu.VMEM)
ANY = pl.BlockSpec(memory_space=pl.ANY)
SMEM = pl.BlockSpec(memory_space=pltpu.SMEM)
BIG = pltpu.CompilerParams(vmem_limit_bytes=40 * 2**20)


def scatter_body(routes, weights, upstream, stream, picker, sent, *, experts, capacity):
    toks = upstream.shape[0]
    slots = experts * capacity
    half = capacity // 2
    r0, r1 = routes[0:1, :], routes[1:2, :]
    names = lax.broadcasted_iota(jnp.int32, (experts, toks), 0)
    hot0 = jnp.where(names == r0, 1.0, 0.0)
    hot1 = jnp.where(names == r1, 1.0, 0.0)
    earlier = jnp.where(
        lax.broadcasted_iota(jnp.int32, (toks, toks), 0)
        < lax.broadcasted_iota(jnp.int32, (toks, toks), 1),
        1.0,
        0.0,
    ).astype(BF)
    before = dot((hot0 + hot1).astype(BF), earlier, 1, 0)
    slot0 = r0 * capacity + jnp.sum(before * hot0, axis=0, keepdims=True).astype(jnp.int32)
    slot1 = r1 * capacity + jnp.sum(before * hot1, axis=0, keepdims=True).astype(jnp.int32)
    blocks = 8
    step = blocks * capacity

    def rows_at(j, carry):
        at = j * (step // 2)
        ids = lax.broadcasted_iota(jnp.int32, (step // 2, toks), 0) + at
        one = jnp.where(ids == slot0, 1.0, 0.0) + jnp.where(ids == slot1, 1.0, 0.0)
        picker[pl.ds(pl.multiple_of(at, step // 2), step // 2), :] = one.astype(BF)
        wide = lax.broadcasted_iota(jnp.int32, (step, toks), 0)
        block = lax.shift_right_logical(wide * (65536 // capacity + 1), 16)
        place = wide - block * capacity
        ids = jnp.where(place >= half, place - half, place) + (block + j * blocks) * half
        hit0, hit1 = ids == slot0, ids == slot1
        pick = (jnp.where(hit0, 1.0, 0.0) + jnp.where(hit1, 1.0, 0.0)).astype(BF)
        weight = jnp.sum(
            jnp.where(hit0, weights[0:1, :], 0.0) + jnp.where(hit1, weights[1:2, :], 0.0),
            axis=1,
            keepdims=True,
        )
        is_cot = place[:, 0:1] >= half
        value = jnp.where(
            is_cot, dot(pick, upstream[...], 1, 0) * weight, dot(pick, stream[...], 1, 0)
        )
        sent[pl.ds(pl.multiple_of(j * step, step), step), :] = value.astype(BF)
        return carry

    lax.fori_loop(0, 2 * slots // step, rows_at, 0)


def offset_of(k, n):
    h = n // 2
    return jnp.where(k < h, jnp.where(k == 0, 0, n - k), jnp.where(k == n - 1, h, k - h + 1))


def load_all(pairs, sems):
    copies = [pltpu.make_async_copy(a, b, sems.at[i]) for i, (a, b) in enumerate(pairs)]
    for copy in copies:
        copy.start()
    for copy in copies:
        copy.wait()


def project_body(z, *refs, n):
    blocks, refs = refs[: n - 1], refs[n - 1 :]
    guo, gux, dno, dnx, gains, inv, own, oth, back, xs = refs[:10]
    buf, guo_v, gux_v, dno_v, dnx_v, sems = refs[10:]
    rows, width = own.shape[0], buf.shape[2]
    hid = dno.shape[0]
    load_all(
        [(guo, guo_v), (gux, gux_v), (dno, dno_v), (dnx, dnx_v)]
        + [(blocks[i], buf.at[i]) for i in range(n - 1)],
        sems,
    )
    own[...] = jnp.zeros(own.shape, F4)
    oth[...] = jnp.zeros(oth.shape, F4)
    back[...] = jnp.zeros(back.shape, F4)

    def step(k, carry):
        chip = lax.rem(z[0] + offset_of(k, n), n)
        at = pl.multiple_of(chip * width, width)
        x = buf[k, :rows, :].astype(F4)
        x = (gains[pl.ds(chip, 1), :] * x * inv[...]).astype(BF)
        xs[pl.ds(pl.multiple_of(k * rows, rows), rows), :] = x
        own[...] += dot(x, guo_v[pl.ds(at, width), :], 1, 0)
        oth[...] += dot(x, gux_v[pl.ds(at, width), :], 1, 0)
        c = buf[k, rows:, :]
        back[:, :hid] += dot(c, dno_v[:, pl.ds(at, width)], 1, 1)
        back[:, hid:] += dot(c, dnx_v[:, pl.ds(at, width)], 1, 1)
        return carry

    lax.fori_loop(0, n - 1, step, 0)


def in_parts(row):
    hi = row.astype(BF).astype(F4)
    mid = (row - hi).astype(BF).astype(F4)
    low = (row - hi - mid).astype(BF).astype(F4)
    return hi, mid, low


def part_rows(row):
    hi, mid, low = in_parts(row)
    shape = (16, row.shape[1])
    at = lax.broadcasted_iota(jnp.int32, shape, 0)
    rows = jnp.where(at == 0, hi, jnp.where(at == 1, mid, jnp.where(at == 2, low, 0.0)))
    return rows.astype(BF)


def whole_row(rows):
    rows = rows.astype(F4)
    return rows[0:1] + rows[1:2] + rows[2:3]


def finish_body(z, xf, cf, guo, gux, dno, dnx, gains, inv, own, oth, back, *refs, n):
    x4, b_own, b_oth, a_own, a_oth, along, send_r, send_l = refs[:8]
    guo_v, gux_v, dno_v, dnx_v, sems = refs[8:]
    rows, width = xf.shape
    hid = dno.shape[0]
    chip = lax.rem(z[0] + n // 2, n)
    at = pl.multiple_of(chip * width, width)
    load_all(
        [
            (guo.at[pl.ds(at, width), :], guo_v),
            (gux.at[pl.ds(at, width), :], gux_v),
            (dno.at[:, pl.ds(at, width)], dno_v),
            (dnx.at[:, pl.ds(at, width)], dnx_v),
        ],
        sems,
    )
    x = (gains[pl.ds(chip, 1), :] * xf[...].astype(F4) * inv[...]).astype(BF)
    x4[...] = x
    total = jnp.zeros((rows, 1), F4)
    for pre, gu_v, dn_v, lo, backs, act in (
        (own, guo_v, dno_v, 0, b_own, a_own),
        (oth, gux_v, dnx_v, hid, b_oth, a_oth),
    ):
        both = pre[...] + dot(x, gu_v[...], 1, 0)
        gate, upper = both[:, :hid], both[:, hid:]
        ab = back[:, lo : lo + hid] + dot(cf[...], dn_v[...], 1, 1)
        sig = jax.nn.sigmoid(gate)
        silu = gate * sig
        act[...] = (silu * upper).astype(BF)
        gb = (ab * upper * (sig * (1.0 + gate * (1.0 - sig)))).astype(BF)
        ub = (ab * silu).astype(BF)
        backs[:, :hid] = gb
        backs[:, hid:] = ub
        total = total + jnp.sum(
            gb.astype(F4) * gate + ub.astype(F4) * upper, axis=1, keepdims=True
        )
    row = jnp.broadcast_to(total, (rows, 128)).T[0:8, :]
    along[:, :rows] = row
    along[:, rows:] = jnp.zeros((8, width - rows), F4)
    part = dot(b_own[...], guo_v[...], 1, 1) + dot(b_oth[...], gux_v[...], 1, 1)
    hr = rows // 2
    send_r[:hr, :] = part[:hr].astype(BF)
    send_r[hr:, :] = part_rows(along[0:1, :])
    send_l[...] = part[hr:].astype(BF)


def parts_body(b_own, b_oth, guo, gux, out):
    out[...] = (dot(b_own[...], guo[...], 1, 1) + dot(b_oth[...], gux[...], 1, 1)).astype(BF)


def hop_body(z, parts, along, ra, la, out_r, out_l, *, k, n, first):
    rows = parts.shape[0]
    width = out_r.shape[1]
    hr = rows // 2

    def block(j):
        at = pl.multiple_of(lax.rem(z[0] + (j + n), n) * width, width)
        return parts[:, pl.ds(at, width)].astype(F4)

    own = along[0:1, :]
    pr, pl_ = block(k), block(-k)
    if first:
        out_r[:hr, :] = (pr[:hr] + ra[:hr, :].astype(F4)).astype(BF)
        out_r[hr:rows, :] = pr[hr:].astype(BF)
        out_r[rows:, :] = part_rows(own + whole_row(ra[hr:, :]))
        out_l[:hr, :] = pl_[:hr].astype(BF)
        out_l[hr:rows, :] = (pl_[hr:] + la[...].astype(F4)).astype(BF)
        out_l[rows:, :] = part_rows(own)
    else:
        out_r[:rows, :] = (pr + ra[:rows, :].astype(F4)).astype(BF)
        out_r[rows:, :] = part_rows(own + whole_row(ra[rows:, :]))
        out_l[:rows, :] = (pl_ + la[:rows, :].astype(F4)).astype(BF)
        out_l[rows:, :] = part_rows(own + whole_row(la[rows:, :]))


def pack_body(z, parts, along, ra, la, out, *, n_sp):
    rows = parts.shape[0]
    width = ra.shape[1]
    half = width // 2
    step = rows // n_sp
    at = pl.multiple_of(z[0] * width, width)
    row = along[0:1, :] + whole_row(ra[rows:, :]) + whole_row(la[rows:, :])
    col = jnp.broadcast_to(row[:, :rows], (128, rows)).T
    hi, mid, low = in_parts(col)
    lane = lax.broadcasted_iota(jnp.int32, (rows, 128), 1)
    extra = jnp.where(lane == 0, hi, jnp.where(lane == 1, mid, jnp.where(lane == 2, low, 0.0)))
    value = (
        parts[:, pl.ds(at, width)].astype(F4) + ra[:rows, :].astype(F4) + la[:rows, :].astype(F4)
    )
    for s in range(n_sp):
        v = value[s * step : (s + 1) * step]
        e = extra[s * step : (s + 1) * step]
        both = jnp.concatenate([v[:, :half], v[:, half:]], axis=0)
        out[2 * s * step : 2 * (s + 1) * step, :half] = both.astype(BF)
        out[2 * s * step : 2 * (s + 1) * step, half:] = jnp.concatenate([e, e], axis=0).astype(BF)


def grads_body(z, *refs, n, add):
    xs, x4 = refs[0], refs[1]
    blocks, cf = refs[2 : n + 1], refs[n + 1]
    backs, act = refs[n + 2], refs[n + 3]
    refs = refs[n + 4 :]
    if add:
        old, gate, up, down, xbuf, cbuf, sems = refs
    else:
        out, xbuf, cbuf, sems = refs
    rows, width = x4.shape
    hid = act.shape[1]
    near = (n - 1) * rows
    load_all(
        [(xs, xbuf.at[pl.ds(0, near), :]), (x4, xbuf.at[pl.ds(near, rows), :])]
        + [
            (blocks[i].at[pl.ds(rows, rows), :], cbuf.at[pl.ds(i * rows, rows), :])
            for i in range(n - 1)
        ]
        + [(cf, cbuf.at[pl.ds(near, rows), :])],
        sems,
    )

    def step(k, carry):
        at = pl.multiple_of(lax.rem(z[0] + offset_of(k, n), n) * width, width)
        mine = pl.ds(pl.multiple_of(k * rows, rows), rows)
        pair = dot(xbuf[mine, :], backs[...], 0, 0)
        dn = dot(act[...], cbuf[mine, :], 0, 0)
        if add:
            gate[pl.ds(at, width), :] = pair[:, :hid] + old[0, pl.ds(at, width), :].astype(F4)
            up[pl.ds(at, width), :] = pair[:, hid:] + old[1, pl.ds(at, width), :].astype(F4)
            for q in range(width // hid):
                lo = pl.multiple_of(at + q * hid, hid)
                down[:, pl.ds(lo, hid)] = dn[:, q * hid : (q + 1) * hid] + old[
                    2, pl.ds(lo, hid), :
                ].astype(F4)
        else:
            out[0, pl.ds(at, width), :] = pair[:, :hid].astype(BF)
            out[1, pl.ds(at, width), :] = pair[:, hid:].astype(BF)
            for q in range(width // hid):
                lo = pl.multiple_of(at + q * hid, hid)
                out[2, pl.ds(lo, hid), :] = dn[:, q * hid : (q + 1) * hid].astype(BF)
        return carry

    lax.fori_loop(0, n, step, 0)


def grads(z, xs, x4, blocks, cf, backs, act, old):
    rows, width = x4.shape
    n, hid = len(blocks) + 1, act.shape[1]
    add = old is not None
    total = n * width
    args = [z, xs, x4, *blocks, cf, backs, act] + ([old] if add else [])
    if add:
        out_shape = tuple(
            jax.ShapeDtypeStruct(t, F4) for t in ((total, hid), (total, hid), (hid, total))
        )
        out_specs = (VMEM,) * 3
    else:
        out_shape, out_specs = jax.ShapeDtypeStruct((3, total, hid), BF), VMEM
    return pl.pallas_call(
        lambda *r: grads_body(*r, n=n, add=add),
        out_shape=out_shape,
        in_specs=[SMEM] + [ANY] * (n + 2) + [VMEM] * (3 if add else 2),
        out_specs=out_specs,
        scratch_shapes=[
            pltpu.VMEM((n * rows, width), BF),
            pltpu.VMEM((n * rows, width), BF),
            pltpu.SemaphoreType.DMA((n + 2,)),
        ],
        compiler_params=BIG,
        cost_estimate=pl.CostEstimate(
            flops=8 * rows * total * 3 * hid, transcendentals=0, bytes_accessed=16 * 2**20
        ),
        name="grads_own" if add else "grads_other",
    )(*args)


def stack_body(*refs):
    refs, sems = refs[:-1], refs[-1]
    srcs, out = refs[:-1], refs[-1]
    pairs, at = [], 0
    flat = out.reshape(out.shape[0] * out.shape[1], out.shape[2])
    for src in srcs:
        pairs.append((src, flat.at[pl.ds(at, src.shape[0]), :]))
        at += src.shape[0]
    load_all(pairs, sems)


def mixed_body(zc, mine, other, w_out, slope, done, out, *, n):
    del done
    width = mine.shape[2]
    out[...] = jnp.zeros(out.shape, F4)
    for ref, core in ((mine, zc[1]), (other, 1 - zc[1])):
        acc = jnp.zeros(out.shape, F4)
        for k in range(n):
            at = pl.multiple_of((2 * lax.rem(zc[0] + k, n) + core) * width, width)
            acc = acc + dot(ref[k], w_out[:, pl.ds(at, width)], 1, 1)
        out[...] += acc
    out[...] *= slope[...]


def outer_body(zc, mine, other, mixed_t, out, *, n):
    for ref, core in ((mine, zc[1]), (other, 1 - zc[1])):
        for k in range(n):
            out[2 * lax.rem(zc[0] + k, n) + core] = dot(mixed_t[...], ref[k], 1, 0).astype(BF)


def conv_body(back, rim, taps, value_in, gate_in, value_grad, gate_grad, padded):
    toks, n_taps = back.shape[0], taps.shape[0]
    padded[:toks, :] = back[...]
    padded[toks:, :] = rim[...]
    step = 64
    for at in range(0, toks, step):
        acc = jnp.zeros((step, back.shape[1]), F4)
        for tap in range(n_taps):
            lo = at + n_taps - 1 - tap
            acc = acc + taps[tap : tap + 1, :] * padded[lo : lo + step, :]
        sigma = jax.nn.sigmoid(gate_in[at : at + step, :].astype(F4))
        value = acc * sigma
        value_grad[at : at + step, :] = value.astype(BF)
        gate_grad[at : at + step, :] = (
            value * value_in[at : at + step, :].astype(F4) * (1.0 - sigma)
        ).astype(BF)


def per_device(
    upstream,
    stream,
    norm_gain,
    routes,
    route_weights,
    w_gate,
    w_up,
    w_down,
    value_in,
    gate_in,
    conv_pre,
    ln_gain,
    conv_taps,
    w_out,
):
    tok_rows, width_part = stream.shape
    n_sp = lax.axis_size("sp")
    n_z = lax.axis_size("z")
    n_tp = 2 * n_z
    z = lax.axis_index("z")
    core = lax.axis_index("c")
    model_width = width_part * n_tp
    channels = conv_pre.shape[1] * n_tp
    tap_count = conv_taps.shape[0]
    capacity = 3 * tok_rows // n_sp
    half_cap = capacity // 2
    experts = n_sp
    slot_count = experts * capacity
    rows = n_sp * half_cap
    wide = 2 * width_part

    zs = z.astype(jnp.int32).reshape(1)
    half = n_z // 2
    hid = w_gate.shape[2]

    picker, sent = pl.pallas_call(
        lambda *r: scatter_body(*r, experts=experts, capacity=capacity),
        out_shape=(
            jax.ShapeDtypeStruct((slot_count, tok_rows), BF),
            jax.ShapeDtypeStruct((2 * slot_count, width_part), BF),
        ),
        in_specs=[VMEM] * 4,
        out_specs=(VMEM, VMEM),
        compiler_params=BIG,
        name="scatter",
    )(routes.T, route_weights.T, upstream, stream)
    arrived = lax.all_to_all(
        sent.reshape(2 * experts, capacity, width_part), ("sp", "c"), 0, 0, tiled=True
    )
    arrived = arrived.reshape(n_sp, 2, 2, half_cap, width_part)
    b0 = jnp.transpose(arrived, (2, 0, 3, 1, 4)).reshape(2 * rows, wide)

    gu_own = jnp.concatenate([w_gate[0], w_up[0]], axis=1)
    down_own = w_down[0]
    gu_oth, down_oth = swap(gu_own), swap(down_own)

    r1, l1 = right(b0), left(b0)
    r2, l2 = right(r1), left(l1)
    r3, l3 = right(r2), left(l2)
    xf, cf = right(r3[:rows]), left(l3[rows:])

    residual = stream.astype(F4)
    conv_vals = conv_pre.astype(F4)
    own_rows = b0[:rows].astype(F4)
    row_part = jnp.sum(own_rows * own_rows, axis=1)
    nothing = jnp.zeros_like(row_part)
    vector = jnp.concatenate(
        [
            jnp.sum(residual * residual, axis=1),
            jnp.sum(conv_vals, axis=1),
            jnp.sum(conv_vals * conv_vals, axis=1),
            jnp.where(core == 0, row_part, nothing),
            jnp.where(core == 0, nothing, row_part),
            norm_gain,
        ]
    )
    told = lax.all_to_all(
        jnp.broadcast_to(vector[None, None], (n_tp, 1, vector.size)), TP, 0, 0, tiled=True
    )[:, 0]
    cut = 3 * tok_rows + 2 * rows
    total = jnp.sum(told[:, :cut], axis=0)
    gains = told[:, cut:].reshape(n_z, wide)
    row_squares, conv_total, conv_squares = jnp.split(total[: 3 * tok_rows], 3)
    slot_squares = jnp.where(
        core == 0, total[3 * tok_rows : 3 * tok_rows + rows], total[3 * tok_rows + rows :]
    )
    inverse = lax.rsqrt(row_squares / model_width + EPSILON)[:, None]
    slot_inverse = lax.rsqrt(slot_squares / model_width + EPSILON)[:, None]

    blocks = [b0, r1, r2, r3, l1, l2, l3]
    weights = (gu_own, gu_oth, down_own, down_oth)
    own, oth, back, xs = pl.pallas_call(
        lambda *r: project_body(*r, n=n_z),
        out_shape=(
            jax.ShapeDtypeStruct((rows, 2 * hid), F4),
            jax.ShapeDtypeStruct((rows, 2 * hid), F4),
            jax.ShapeDtypeStruct((rows, 2 * hid), F4),
            jax.ShapeDtypeStruct(((n_z - 1) * rows, wide), BF),
        ),
        in_specs=[SMEM] + [ANY] * (n_z - 1 + 4) + [VMEM] * 2,
        out_specs=(VMEM,) * 4,
        scratch_shapes=[
            pltpu.VMEM((n_z - 1, 2 * rows, wide), BF),
            pltpu.VMEM(gu_own.shape, BF),
            pltpu.VMEM(gu_own.shape, BF),
            pltpu.VMEM(down_own.shape, BF),
            pltpu.VMEM(down_own.shape, BF),
            pltpu.SemaphoreType.DMA((n_z + 3,)),
        ],
        compiler_params=BIG,
        name="project",
    )(zs, *blocks, *weights, gains, slot_inverse)

    x4, b_own, b_oth, a_own, a_oth, along, ra, la = pl.pallas_call(
        lambda *r: finish_body(*r, n=n_z),
        out_shape=(
            jax.ShapeDtypeStruct((rows, wide), BF),
            jax.ShapeDtypeStruct((rows, 2 * hid), BF),
            jax.ShapeDtypeStruct((rows, 2 * hid), BF),
            jax.ShapeDtypeStruct((rows, hid), BF),
            jax.ShapeDtypeStruct((rows, hid), BF),
            jax.ShapeDtypeStruct((8, wide), F4),
            jax.ShapeDtypeStruct((rows // 2 + 16, wide), BF),
            jax.ShapeDtypeStruct((rows // 2, wide), BF),
        ),
        in_specs=[SMEM] + [VMEM] * 2 + [ANY] * 4 + [VMEM] * 5,
        out_specs=(VMEM,) * 8,
        scratch_shapes=[
            pltpu.VMEM((wide, 2 * hid), BF),
            pltpu.VMEM((wide, 2 * hid), BF),
            pltpu.VMEM((hid, wide), BF),
            pltpu.VMEM((hid, wide), BF),
            pltpu.SemaphoreType.DMA((4,)),
        ],
        compiler_params=BIG,
        name="finish",
    )(zs, xf, cf, *weights, gains, slot_inverse, own, oth, back)

    ra, la = right(ra), left(la)
    parts = pl.pallas_call(
        parts_body,
        grid=(n_z,),
        out_shape=jax.ShapeDtypeStruct((rows, model_width), BF),
        in_specs=[
            pl.BlockSpec((rows, 2 * hid), lambda i: (0, 0)),
            pl.BlockSpec((rows, 2 * hid), lambda i: (0, 0)),
            pl.BlockSpec((wide, 2 * hid), lambda i: (i, 0)),
            pl.BlockSpec((wide, 2 * hid), lambda i: (i, 0)),
        ],
        out_specs=pl.BlockSpec((rows, wide), lambda i: (0, i)),
        name="parts",
    )(b_own, b_oth, gu_own, gu_oth)
    message = jax.ShapeDtypeStruct((rows + 16, wide), BF)
    for k in range(half - 1, 0, -1):
        ra, la = pl.pallas_call(
            lambda *r, k=k: hop_body(*r, k=k, n=n_z, first=k == half - 1),
            out_shape=(message, message),
            in_specs=[SMEM] + [VMEM] * 4,
            out_specs=(VMEM, VMEM),
            compiler_params=BIG,
            name="hop",
        )(zs, parts, along, ra, la)
        ra, la = right(ra), left(la)
    sent_back = pl.pallas_call(
        lambda *r: pack_body(*r, n_sp=n_sp),
        out_shape=jax.ShapeDtypeStruct((slot_count, width_part + 128), BF),
        in_specs=[SMEM] + [VMEM] * 4,
        out_specs=VMEM,
        compiler_params=BIG,
        name="pack",
    )(zs, parts, along, ra, la)
    returned = lax.all_to_all(
        sent_back.reshape(2 * n_sp, half_cap, width_part + 128), ("sp", "c"), 0, 0, tiled=True
    ).reshape(slot_count, width_part + 128)

    others = grads(zs, xs, x4, blocks, cf, b_oth, a_oth, None)
    returned, others = lax.optimization_barrier((returned, others))
    grad_gate, grad_up, grad_down = grads(
        zs, xs, x4, blocks, cf, b_own, a_own, swap(others)
    )

    token_back = dot(picker, returned, 0, 0)
    inner = jnp.sum(token_back[:, width_part : width_part + 3], axis=1, keepdims=True)
    gained = norm_gain[None, :] * token_back[:, :width_part]
    norm_back = inverse * gained - residual * inverse**2 * (inner / model_width)
    stream_grad = (upstream.astype(F4) + norm_back).astype(BF)

    ht = tok_rows // 2
    p1, m1, p2, m2 = (hops(stream_grad, d) for d in (1, -1, 2, -2))
    p3, m3 = hops(p1, 2), hops(m1, -2)
    pf, mf = hops(p2[:ht], 2), hops(m2[ht:], -2)
    mine8 = pl.pallas_call(
        stack_body,
        out_shape=jax.ShapeDtypeStruct((n_z, tok_rows, width_part), BF),
        in_specs=[ANY] * 9,
        out_specs=ANY,
        scratch_shapes=[pltpu.SemaphoreType.DMA((9,))],
        name="stack",
    )(stream_grad, m1, m2, m3, pf, mf, p3, p2, p1)
    other8 = swap(mine8)

    mean_val = (conv_total / channels)[:, None]
    variance = (conv_squares / channels)[:, None] - mean_val * mean_val
    inv_std = lax.rsqrt(variance + EPSILON)
    centred = (conv_vals - mean_val) * inv_std
    scaled = centred * ln_gain[None, :]
    mixed_out = jax.nn.silu(scaled).astype(BF)

    zc = jnp.stack([z, core]).astype(jnp.int32)
    slope = silu_slope(scaled) * ln_gain[None, :]
    norm_in = pl.pallas_call(
        lambda *r: mixed_body(*r, n=n_z),
        out_shape=jax.ShapeDtypeStruct(conv_pre.shape, F4),
        in_specs=[SMEM] + [VMEM] * 4 + [ANY],
        out_specs=VMEM,
        compiler_params=BIG,
        name="mixed",
    )(zc, mine8, other8, w_out, slope, grad_gate)
    out_parts = pl.pallas_call(
        lambda *r: outer_body(*r, n=n_z),
        out_shape=jax.ShapeDtypeStruct((n_sp, conv_pre.shape[1], width_part), BF),
        in_specs=[SMEM] + [VMEM] * 3,
        out_specs=VMEM,
        compiler_params=BIG,
        name="outer",
    )(zc, mine8, other8, mixed_out.T)
    norm_total, norm_cross = in_one((jnp.sum(norm_in, axis=1), jnp.sum(norm_in * centred, axis=1)))
    conv_back = inv_std * (
        norm_in - (norm_total / channels)[:, None] - centred * (norm_cross / channels)[:, None]
    )
    next_rim = lax.ppermute(conv_back[:32], "sp", [(i + 1, i) for i in range(n_sp - 1)])
    grad_out = jnp.sum(
        lax.all_to_all(out_parts, "sp", 0, 0, tiled=True).astype(F4), axis=0
    )
    value_grad, gate_grad = pl.pallas_call(
        conv_body,
        out_shape=(jax.ShapeDtypeStruct(value_in.shape, BF),) * 2,
        in_specs=[VMEM] * 5,
        out_specs=(VMEM, VMEM),
        scratch_shapes=[pltpu.VMEM((tok_rows + 32, conv_pre.shape[1]), F4)],
        name="conv",
    )(conv_back, next_rim, conv_taps, value_in, gate_in)
    return (grad_gate[None], grad_up[None], grad_down[None], grad_out, value_grad, gate_grad)


def solution(mesh):
    n_sp, n_tp = mesh.devices.shape
    split = Mesh(mesh.devices.reshape(n_sp, n_tp // 2, 2), ("sp", "z", "c"))
    return jax.shard_map(
        per_device,
        mesh=split,
        in_specs=(
            P("sp", TP),
            P("sp", TP),
            P(TP),
            P("sp", None),
            P("sp", None),
            P("sp", None, TP),
            P("sp", None, TP),
            P("sp", TP, None),
            P("sp", TP),
            P("sp", TP),
            P("sp", TP),
            P(TP),
            P(None, TP),
            P(TP, None),
        ),
        out_specs=(
            P("sp", None, TP),
            P("sp", None, TP),
            P("sp", TP, None),
            P(TP, "sp"),
            P("sp", TP),
            P("sp", TP),
        ),
        check_vma=False,
    )
```

profile of v0, /device:TPU:1, one launch (start us, length us, event | category | flops | bytes accessed | tf_op | source)
XLA Modules:
  0.0 298.1 jit_solution(18413570964705123935)
XLA Ops:
  5.5 22.8 %all_to_all.26 = bf16[32,48,256]{2,1,0:T(8,128)(2,1)S(1)} all-to-all(bf16[32,48,256]{2,1,0:T(8,128)(2,1)S(1)} %bitcast.35), channel_id=1, replica_groups=mesh['sp'=16,'z'=8,'c'=2] {'sp','c'}, dimensions={0} | all-to-all | bytes 1572864 | tf_op jit(solution)/shard_map/all_to_all | solution.py:444
  30.8 4.0 %collective-permute-start.3 = (bf16[768,512]{1,0:T(8,128)(2,1)S(1)}, bf16[768,512]{1,0:T(8,128)(2,1)}, u32[]{:S(2)}, u32[]{:S(2)}) collective-permute-start(bf16[768,512]{1,0:T(8,128)(2,1)S(1)} %bitcast.30), channel_id=1, source_target_pairs={{0,14},{2,0},{4,2},{6,4},{8,6},{10,8},{12,10},{14,12},{1,15},{3,1}... | collective-permute-start | bytes 2359304 | tf_op jit(solution)/shard_map/ppermute | solution.py:38
  36.0 16.2 %collective-permute-done.r_2_.r_4_ = bf16[768,512]{1,0:T(8,128)(2,1)} collective-permute-done((bf16[768,512]{1,0:T(8,128)(2,1)S(1)}, bf16[768,512]{1,0:T(8,128)(2,1)}, u32[]{:S(2)}, u32[]{:S(2)}) %collective-permute-start) | collective-permute-done | bytes 786464 | tf_op jit(solution)/shard_map/ppermute | solution.py:33
  52.2 2.7 collective-permute-start.4
  56.9 14.9 %collective-permute-done.1.r_3_.r_5_ = bf16[768,512]{1,0:T(8,128)(2,1)} collective-permute-done((bf16[768,512]{1,0:T(8,128)(2,1)}, bf16[768,512]{1,0:T(8,128)(2,1)}, u32[]{:S(2)}, u32[]{:S(2)}) %collective-permute-start.1) | collective-permute-done | bytes 786464 | tf_op jit(solution)/shard_map/ppermute | solution.py:33
  71.7 2.7 collective-permute-start.5
  76.5 7.8 %all-to-all-start.1 = ((f32[16,1,1792]{2,1,0:T(1,128)}), f32[16,1,1792]{2,1,0:T(1,128)S(1)}, u32[]{:S(2)}, u32[]{:S(2)}) async-start(f32[16,1,1792]{2,1,0:T(1,128)} %broadcast_in_dim.15), calls=%async_computation.1 | async-start | bytes 229376 | tf_op jit(solution)/shard_map/all_to_all | solution.py:474
  84.3 6.7 %collective-permute-done.2.r_4_.r_6_ = bf16[768,512]{1,0:T(8,128)(2,1)} collective-permute-done((bf16[768,512]{1,0:T(8,128)(2,1)}, bf16[768,512]{1,0:T(8,128)(2,1)}, u32[]{:S(2)}, u32[]{:S(2)}) %collective-permute-start.2) | collective-permute-done | bytes 786464 | tf_op jit(solution)/shard_map/ppermute | solution.py:33
  94.6 2.7 collective-permute-start.9
  98.6 9.2 %project.1 = (f32[384,256]{1,0:T(8,128)S(1)}, f32[384,256]{1,0:T(8,128)S(1)}, f32[384,256]{1,0:T(8,128)S(1)}, bf16[2688,512]{1,0:T(8,128)(2,1)}) custom-call(s32[1]{0:T(128)} %bitcast.r_0_, bf16[768,512]{1,0:T(8,128)(2,1)S(1)} %bitcast.31, bf16[768,512]{1,0:T(8,128)(2,1)} %collective-permute-done.r_2_.r_4_, ...), custom_call_target="tpu_custom_call" | custom-call | tf_op jit(solution)/shard_map/project/pallas_call | solution.py:489
  107.9 3.8 %finish.1 = (bf16[384,512]{1,0:T(8,128)(2,1)S(1)}, bf16[384,256]{1,0:T(8,128)(2,1)S(1)}, bf16[384,256]{1,0:T(8,128)(2,1)S(1)}, bf16[384,128]{1,0:T(8,128)(2,1)S(...) custom-call(s32[1]{0:T(128)} %bitcast.r_0_, ...), custom_call_target="tpu_custom_call" | custom-call | tf_op jit(solution)/shard_map/finish/pallas_call | solution.py:511
  117.8 7.8 %parts.1.r_1_ = bf16[384,4096]{1,0:T(8,128)(2,1)} custom-call(bf16[384,256]{1,0:T(8,128)(2,1)} %copy-done.15, bf16[384,256]{1,0:T(8,128)(2,1)} %copy-done.17, bf16[4096,256]{1,0:T(8,128)(2,1)} %copy-done.1, bf16[4096,256]{1,0:T(8,128)(2,1)} %collective-permute-done.6.r_9_.r_4_.gux), custom_call_target="tpu_custom_call" | custom-call | tf_op jit(solution)/shard_map/parts/pallas_call | solution.py:537
  127.8 2.6 collective-permute-start.13
  130.4 5.3 %collective-permute-done.12.r_3_ = bf16[400,512]{1,0:T(8,128)(2,1)S(1)} collective-permute-done((bf16[400,512]{1,0:T(8,128)(2,1)S(1)}, bf16[400,512]{1,0:T(8,128)(2,1)S(1)}, u32[]{:S(2)}, u32[]{:S(2)}) %collective-permute-start.12) | collective-permute-done | bytes 409632 | tf_op jit(solution)/shard_map/ppermute | solution.py:33
  136.1 2.8 collective-permute-start.15
  138.8 6.9 %collective-permute-done.14.r_3_ = bf16[400,512]{1,0:T(8,128)(2,1)S(1)} collective-permute-done((bf16[400,512]{1,0:T(8,128)(2,1)S(1)}, bf16[400,512]{1,0:T(8,128)(2,1)S(1)}, u32[]{:S(2)}, u32[]{:S(2)}) %collective-permute-start.14) | collective-permute-done | bytes 409632 | tf_op jit(solution)/shard_map/ppermute | solution.py:33
  146.1 3.0 %collective-permute-start.17 = (bf16[400,512]{1,0:T(8,128)(2,1)S(1)}, bf16[400,512]{1,0:T(8,128)(2,1)S(1)}, u32[]{:S(2)}, u32[]{:S(2)}) collective-permute-start(bf16[400,512]{1,0:T(8,128)(2,1)S(1)} %get-tuple-element.50), channel_id=1, source_target_pairs={{0,14},{2,0},{4,2},{6,4},{8,6},{10,8},{12,10},{14,12},{1,15},{3,1}... | collective-permute-start | bytes 1228808 | tf_op jit(solution)/shard_map/ppermute | solution.py:38
  149.1 8.0 %collective-permute-done.16.r_3_ = bf16[400,512]{1,0:T(8,128)(2,1)S(1)} collective-permute-done((bf16[400,512]{1,0:T(8,128)(2,1)S(1)}, bf16[400,512]{1,0:T(8,128)(2,1)S(1)}, u32[]{:S(2)}, u32[]{:S(2)}) %collective-permute-start.16) | collective-permute-done | bytes 409632 | tf_op jit(solution)/shard_map/ppermute | solution.py:33
  158.3 14.4 %all-to-all-start.2 = ((bf16[32,24,384]{2,1,0:T(8,128)(2,1)}), bf16[32,24,384]{2,1,0:T(8,128)(2,1)S(1)}, u32[]{:S(2)}, u32[]{:S(2)}) async-start(bf16[32,24,384]{2,1,0:T(8,128)(2,1)} %bitcast.10), calls=%async_computation.2 | async-start | bytes 1179648 | tf_op jit(solution)/shard_map/all_to_all | solution.py:569
  174.6 5.9 %grads_other.1 = bf16[3,4096,128]{2,1,0:T(8,128)(2,1)S(1)} custom-call(s32[1]{0:T(128)} %bitcast.r_0_, bf16[2688,512]{1,0:T(8,128)(2,1)S(1)} %copy-done.22, bf16[384,512]{1,0:T(8,128)(2,1)S(1)} %copy-done.25, bf16[768,512]{1,0:T(8,128)(2,1)S(1)} %bitcast.32, bf16[768,512]{1,0:T(8,128)(2,1)} %collective-permute-done.r_2_.r_4_, ...), custom_call_target="tpu_custom_call" | custom-call | flops 4831838208 | bytes 16777216 | tf_op jit(solution)/shard_map/grads_other/pallas_call | solution.py:331
  182.1 2.9 all-to-all-done.2
  194.2 3.4 %collective-permute-done.22.refs_7_ = bf16[256,256]{1,0:T(8,128)(2,1)S(1)} collective-permute-done((bf16[256,256]{1,0:T(8,128)(2,1)S(1)}, bf16[256,256]{1,0:T(8,128)(2,1)S(1)}, u32[]{:S(2)}, u32[]{:S(2)}) %collective-permute-start.22) | collective-permute-done | bytes 131104 | tf_op jit(solution)/shard_map/ppermute | solution.py:43
  198.7 2.6 collective-permute-start.24
  201.3 4.1 %collective-permute-done.23.refs_4_ = bf16[128,256]{1,0:T(8,128)(2,1)S(1)} collective-permute-done((bf16[128,256]{1,0:T(8,128)(2,1)S(1)}, bf16[128,256]{1,0:T(8,128)(2,1)S(1)}, u32[]{:S(2)}, u32[]{:S(2)}) %collective-permute-start.23) | collective-permute-done | bytes 65568 | tf_op jit(solution)/shard_map/ppermute | solution.py:43
  207.4 32.9 %stack.10.r_1_ = bf16[8,256,256]{2,1,0:T(8,128)(2,1)} custom-call(bf16[256,256]{1,0:T(8,128)(2,1)} %copy-done.37, bf16[256,256]{1,0:T(8,128)(2,1)} %copy-done.40, bf16[256,256]{1,0:T(8,128)(2,1)} %copy-done.39, bf16[256,256]{1,0:T(8,128)(2,1)} %copy-done.42, bf16[128,256]{1,0:T(8,128)(2,1)} %copy-done.44, bf16[128,256]{1,0:T(8,128)(2,1)} %copy-done.45, ...), custom_call_target="tpu_custom_call" | custom-call | tf_op jit(solution)/shard_map/stack/pallas_call | solution.py:589
  240.3 2.6 collective-permute-start.27
  246.0 10.6 %grads_own.1 = (f32[4096,128]{1,0:T(8,128)}, f32[4096,128]{1,0:T(8,128)}, f32[128,4096]{1,0:T(8,128)}) custom-call(s32[1]{0:T(128)} %bitcast.r_0_, bf16[2688,512]{1,0:T(8,128)(2,1)S(1)} %copy-done.23, bf16[384,512]{1,0:T(8,128)(2,1)S(1)} %copy-done.26, bf16[768,512]{1,0:T(8,128)(2,1)S(1)} %bitcast.33, bf16[768,512]{1,0:T(8,128)(2,1)} %collective-permute-done.r_2_.r_4_, ...), custom_call_target="tpu_custom_call" | custom-call | flops 4831838208 | bytes 16777216 | tf_op jit(solution)/shard_map/grads_own/pallas_call | solution.py:331
  260.4 6.7 %all-to-all-start.4 = ((f32[16,1,512]{2,1,0:T(1,128)}), f32[16,1,512]{2,1,0:T(1,128)S(1)}, u32[]{:S(2)}, u32[]{:S(2)}) async-start(f32[16,1,512]{2,1,0:T(1,128)} %broadcast_in_dim.20), calls=%async_computation.4 | async-start | bytes 65536 | tf_op jit(solution)/shard_map/all_to_all | solution.py:16
  267.3 2.0 outer.1
  269.3 5.2 %all-to-all-done.4 = f32[16,1,512]{2,1,0:T(1,128)S(1)} async-done(((f32[16,1,512]{2,1,0:T(1,128)}), f32[16,1,512]{2,1,0:T(1,128)S(1)}, u32[]{:S(2)}, u32[]{:S(2)}) %all-to-all-start.4) | async-done | bytes 32800 | tf_op jit(solution)/shard_map/all_to_all | solution.py:16
  274.5 3.9 %all-to-all-start.3 = ((bf16[16,128,256]{2,1,0:T(8,128)(2,1)}), bf16[16,128,256]{2,1,0:T(8,128)(2,1)S(1)}, u32[]{:S(2)}, u32[]{:S(2)}) async-start(bf16[16,128,256]{2,1,0:T(8,128)(2,1)} %outer.1), calls=%async_computation.3 | async-start | bytes 2097152 | tf_op jit(solution)/shard_map/all_to_all | solution.py:630
  280.0 14.7 %all-to-all-done.3 = bf16[16,128,256]{2,1,0:T(8,128)(2,1)S(1)} async-done(((bf16[16,128,256]{2,1,0:T(8,128)(2,1)}), bf16[16,128,256]{2,1,0:T(8,128)(2,1)S(1)}, u32[]{:S(2)}, u32[]{:S(2)}) %all-to-all-start.3) | async-done | bytes 1048608 | tf_op jit(solution)/shard_map/all_to_all | solution.py:630
  (190 shorter events, 54.7 us)
Async XLA Ops:
  29.0 23.2 %collective-permute-start = (bf16[768,512]{1,0:T(8,128)(2,1)S(1)}, bf16[768,512]{1,0:T(8,128)(2,1)}, u32[]{:S(2)}, u32[]{:S(2)}) collective-permute-start(bf16[768,512]{1,0:T(8,128)(2,1)S(1)} %bitcast.29), channel_id=1, source_target_pairs={{0,2},{2,4},{4,6},{6,8},{8,10},{10,12},{12,14},{14,0},{1,3},{3,5},... | collective-permute-start | bytes 2359304 | tf_op jit(solution)/shard_map/ppermute | solution.py:33
  30.8 21.4 %collective-permute-start.3 = (bf16[768,512]{1,0:T(8,128)(2,1)S(1)}, bf16[768,512]{1,0:T(8,128)(2,1)}, u32[]{:S(2)}, u32[]{:S(2)}) collective-permute-start(bf16[768,512]{1,0:T(8,128)(2,1)S(1)} %bitcast.30), channel_id=1, source_target_pairs={{0,14},{2,0},{4,2},{6,4},{8,6},{10,8},{12,10},{14,12},{1,15},{3,1}... | collective-permute-start | bytes 2359304 | tf_op jit(solution)/shard_map/ppermute | solution.py:38
  35.1 62.4 %collective-permute-start.6 = (bf16[4096,256]{1,0:T(8,128)(2,1)S(1)}, bf16[4096,256]{1,0:T(8,128)(2,1)}, u32[]{:S(2)}, u32[]{:S(2)}) collective-permute-start(bf16[4096,256]{1,0:T(8,128)(2,1)S(1)} %pad_maximum_fusion.r_8_.r_3_.guo), channel_id=1, source_target_pairs={{0,1},{1,0},{2,3},{3,2},{4,5},{5,4},{6,7},{7,6},{8,9},{9,8},{10,11... | collective-permute-start | bytes 6291464 | tf_op jit(solution)/shard_map/ppermute | solution.py:47
  52.2 19.5 %collective-permute-start.1 = (bf16[768,512]{1,0:T(8,128)(2,1)}, bf16[768,512]{1,0:T(8,128)(2,1)}, u32[]{:S(2)}, u32[]{:S(2)}) collective-permute-start(bf16[768,512]{1,0:T(8,128)(2,1)} %collective-permute-done.r_2_.r_4_), channel_id=1, source_target_pairs={{0,2},{2,4},{4,6},{6,8},{8,10},{10,12},{12,14},{14,0},{1,3},{3,5},... | collective-permute-start | bytes 2359304 | tf_op jit(solution)/shard_map/ppermute | solution.py:33
  52.2 19.5 %collective-permute-start.4 = (bf16[768,512]{1,0:T(8,128)(2,1)}, bf16[768,512]{1,0:T(8,128)(2,1)}, u32[]{:S(2)}, u32[]{:S(2)}) collective-permute-start(bf16[768,512]{1,0:T(8,128)(2,1)} %collective-permute-done.3.r_5_.r_7_), channel_id=1, source_target_pairs={{0,14},{2,0},{4,2},{6,4},{8,6},{10,8},{12,10},{14,12},{1,15},{3,1}... | collective-permute-start | bytes 2359304 | tf_op jit(solution)/shard_map/ppermute | solution.py:38
  54.9 42.6 %collective-permute-start.7 = (bf16[128,4096]{1,0:T(8,128)(2,1)S(1)}, bf16[128,4096]{1,0:T(8,128)(2,1)}, u32[]{:S(2)}, u32[]{:S(2)}) collective-permute-start(bf16[128,4096]{1,0:T(8,128)(2,1)S(1)} %bitcast.26), channel_id=1, source_target_pairs={{0,1},{1,0},{2,3},{3,2},{4,5},{5,4},{6,7},{7,6},{8,9},{9,8},{10,11... | collective-permute-start | bytes 3145736 | tf_op jit(solution)/shard_map/ppermute | solution.py:47
  71.7 19.3 %collective-permute-start.2 = (bf16[768,512]{1,0:T(8,128)(2,1)}, bf16[768,512]{1,0:T(8,128)(2,1)}, u32[]{:S(2)}, u32[]{:S(2)}) collective-permute-start(bf16[768,512]{1,0:T(8,128)(2,1)} %collective-permute-done.1.r_3_.r_5_), channel_id=1, source_target_pairs={{0,2},{2,4},{4,6},{6,8},{8,10},{10,12},{12,14},{14,0},{1,3},{3,5},... | collective-permute-start | bytes 2359304 | tf_op jit(solution)/shard_map/ppermute | solution.py:33
  71.7 21.1 %collective-permute-start.5 = (bf16[768,512]{1,0:T(8,128)(2,1)}, bf16[768,512]{1,0:T(8,128)(2,1)}, u32[]{:S(2)}, u32[]{:S(2)}) collective-permute-start(bf16[768,512]{1,0:T(8,128)(2,1)} %collective-permute-done.4.r_6_.r_8_), channel_id=1, source_target_pairs={{0,14},{2,0},{4,2},{6,4},{8,6},{10,8},{12,10},{14,12},{1,15},{3,1}... | collective-permute-start | bytes 2359304 | tf_op jit(solution)/shard_map/ppermute | solution.py:38
  76.5 20.7 %all-to-all-start.1 = ((f32[16,1,1792]{2,1,0:T(1,128)}), f32[16,1,1792]{2,1,0:T(1,128)S(1)}, u32[]{:S(2)}, u32[]{:S(2)}) async-start(f32[16,1,1792]{2,1,0:T(1,128)} %broadcast_in_dim.15), calls=%async_computation.1 | async-start | bytes 229376 | tf_op jit(solution)/shard_map/all_to_all | solution.py:474
  92.8 15.1 %collective-permute-start.8 = (bf16[384,512]{1,0:T(8,128)(2,1)}, bf16[384,512]{1,0:T(8,128)(2,1)}, u32[]{:S(2)}, u32[]{:S(2)}) collective-permute-start(bf16[384,512]{1,0:T(8,128)(2,1)} %slice.66), channel_id=1, source_target_pairs={{0,2},{2,4},{4,6},{6,8},{8,10},{10,12},{12,14},{14,0},{1,3},{3,5},... | collective-permute-start | bytes 1179656 | tf_op jit(solution)/shard_map/ppermute | solution.py:33
  94.6 13.3 %collective-permute-start.9 = (bf16[384,512]{1,0:T(8,128)(2,1)}, bf16[384,512]{1,0:T(8,128)(2,1)}, u32[]{:S(2)}, u32[]{:S(2)}) collective-permute-start(bf16[384,512]{1,0:T(8,128)(2,1)} %slice.67), channel_id=1, source_target_pairs={{0,14},{2,0},{4,2},{6,4},{8,6},{10,8},{12,10},{14,12},{1,15},{3,1}... | collective-permute-start | bytes 1179656 | tf_op jit(solution)/shard_map/ppermute | solution.py:38
  115.1 10.5 %collective-permute-start.10 = (bf16[208,512]{1,0:T(8,128)(2,1)S(1)}, bf16[208,512]{1,0:T(8,128)(2,1)S(1)}, u32[]{:S(2)}, u32[]{:S(2)}) collective-permute-start(bf16[208,512]{1,0:T(8,128)(2,1)S(1)} %get-tuple-element.43), channel_id=1, source_target_pairs={{0,2},{2,4},{4,6},{6,8},{8,10},{10,12},{12,14},{14,0},{1,3},{3,5},... | collective-permute-start | bytes 638984 | tf_op jit(solution)/shard_map/ppermute | solution.py:33
  116.4 9.2 %collective-permute-start.11 = (bf16[192,512]{1,0:T(8,128)(2,1)}, bf16[192,512]{1,0:T(8,128)(2,1)S(1)}, u32[]{:S(2)}, u32[]{:S(2)}) collective-permute-start(bf16[192,512]{1,0:T(8,128)(2,1)} %get-tuple-element.44), channel_id=1, source_target_pairs={{0,14},{2,0},{4,2},{6,4},{8,6},{10,8},{12,10},{14,12},{1,15},{3,1}... | collective-permute-start | bytes 589832 | tf_op jit(solution)/shard_map/ppermute | solution.py:38
  127.6 8.1 %collective-permute-start.12 = (bf16[400,512]{1,0:T(8,128)(2,1)S(1)}, bf16[400,512]{1,0:T(8,128)(2,1)S(1)}, u32[]{:S(2)}, u32[]{:S(2)}) collective-permute-start(bf16[400,512]{1,0:T(8,128)(2,1)S(1)} %get-tuple-element.45), channel_id=1, source_target_pairs={{0,2},{2,4},{4,6},{6,8},{8,10},{10,12},{12,14},{14,0},{1,3},{3,5},... | collective-permute-start | bytes 1228808 | tf_op jit(solution)/shard_map/ppermute | solution.py:33
  127.8 8.0 %collective-permute-start.13 = (bf16[400,512]{1,0:T(8,128)(2,1)S(1)}, bf16[400,512]{1,0:T(8,128)(2,1)S(1)}, u32[]{:S(2)}, u32[]{:S(2)}) collective-permute-start(bf16[400,512]{1,0:T(8,128)(2,1)S(1)} %get-tuple-element.46), channel_id=1, source_target_pairs={{0,14},{2,0},{4,2},{6,4},{8,6},{10,8},{12,10},{14,12},{1,15},{3,1}... | collective-permute-start | bytes 1228808 | tf_op jit(solution)/shard_map/ppermute | solution.py:38
  136.0 9.8 %collective-permute-start.14 = (bf16[400,512]{1,0:T(8,128)(2,1)S(1)}, bf16[400,512]{1,0:T(8,128)(2,1)S(1)}, u32[]{:S(2)}, u32[]{:S(2)}) collective-permute-start(bf16[400,512]{1,0:T(8,128)(2,1)S(1)} %get-tuple-element.47), channel_id=1, source_target_pairs={{0,2},{2,4},{4,6},{6,8},{8,10},{10,12},{12,14},{14,0},{1,3},{3,5},... | collective-permute-start | bytes 1228808 | tf_op jit(solution)/shard_map/ppermute | solution.py:33
  136.1 9.7 %collective-permute-start.15 = (bf16[400,512]{1,0:T(8,128)(2,1)S(1)}, bf16[400,512]{1,0:T(8,128)(2,1)S(1)}, u32[]{:S(2)}, u32[]{:S(2)}) collective-permute-start(bf16[400,512]{1,0:T(8,128)(2,1)S(1)} %get-tuple-element.48), channel_id=1, source_target_pairs={{0,14},{2,0},{4,2},{6,4},{8,6},{10,8},{12,10},{14,12},{1,15},{3,1}... | collective-permute-start | bytes 1228808 | tf_op jit(solution)/shard_map/ppermute | solution.py:38
  146.0 11.1 %collective-permute-start.16 = (bf16[400,512]{1,0:T(8,128)(2,1)S(1)}, bf16[400,512]{1,0:T(8,128)(2,1)S(1)}, u32[]{:S(2)}, u32[]{:S(2)}) collective-permute-start(bf16[400,512]{1,0:T(8,128)(2,1)S(1)} %get-tuple-element.49), channel_id=1, source_target_pairs={{0,2},{2,4},{4,6},{6,8},{8,10},{10,12},{12,14},{14,0},{1,3},{3,5},... | collective-permute-start | bytes 1228808 | tf_op jit(solution)/shard_map/ppermute | solution.py:33
  146.1 11.0 %collective-permute-start.17 = (bf16[400,512]{1,0:T(8,128)(2,1)S(1)}, bf16[400,512]{1,0:T(8,128)(2,1)S(1)}, u32[]{:S(2)}, u32[]{:S(2)}) collective-permute-start(bf16[400,512]{1,0:T(8,128)(2,1)S(1)} %get-tuple-element.50), channel_id=1, source_target_pairs={{0,14},{2,0},{4,2},{6,4},{8,6},{10,8},{12,10},{14,12},{1,15},{3,1}... | collective-permute-start | bytes 1228808 | tf_op jit(solution)/shard_map/ppermute | solution.py:38
  158.3 26.7 %all-to-all-start.2 = ((bf16[32,24,384]{2,1,0:T(8,128)(2,1)}), bf16[32,24,384]{2,1,0:T(8,128)(2,1)S(1)}, u32[]{:S(2)}, u32[]{:S(2)}) async-start(bf16[32,24,384]{2,1,0:T(8,128)(2,1)} %bitcast.10), calls=%async_computation.2 | async-start | bytes 1179648 | tf_op jit(solution)/shard_map/all_to_all | solution.py:569
  185.0 58.2 %collective-permute-start.18 = (bf16[3,4096,128]{2,1,0:T(8,128)(2,1)}, bf16[3,4096,128]{2,1,0:T(8,128)(2,1)}, u32[]{:S(2)}, u32[]{:S(2)}) collective-permute-start(bf16[3,4096,128]{2,1,0:T(8,128)(2,1)} %copy-done.21), channel_id=1, source_target_pairs={{0,1},{1,0},{2,3},{3,2},{4,5},{5,4},{6,7},{7,6},{8,9},{9,8},{10,11... | collective-permute-start | bytes 9437192 | tf_op jit(solution)/shard_map/ppermute | solution.py:47
  187.3 6.4 %collective-permute-start.25 = (bf16[256,256]{1,0:T(8,128)(2,1)S(1)}, bf16[256,256]{1,0:T(8,128)(2,1)S(1)}, u32[]{:S(2)}, u32[]{:S(2)}) collective-permute-start(bf16[256,256]{1,0:T(8,128)(2,1)S(1)} %fusion.4.refs_0_), channel_id=1, source_target_pairs={{0,2},{2,4},{4,6},{6,8},{8,10},{10,12},{12,14},{14,0},{1,3},{3,5},... | collective-permute-start | bytes 393224 | tf_op jit(solution)/shard_map/ppermute | solution.py:43
  188.1 9.5 %collective-permute-start.22 = (bf16[256,256]{1,0:T(8,128)(2,1)S(1)}, bf16[256,256]{1,0:T(8,128)(2,1)S(1)}, u32[]{:S(2)}, u32[]{:S(2)}) collective-permute-start(bf16[256,256]{1,0:T(8,128)(2,1)S(1)} %fusion.4.refs_0_), channel_id=1, source_target_pairs={{0,4},{2,6},{4,8},{6,10},{8,12},{10,14},{12,0},{14,2},{1,5},{3,7},... | collective-permute-start | bytes 393224 | tf_op jit(solution)/shard_map/ppermute | solution.py:43
  190.0 8.7 %collective-permute-start.20 = (bf16[256,256]{1,0:T(8,128)(2,1)S(1)}, bf16[256,256]{1,0:T(8,128)(2,1)S(1)}, u32[]{:S(2)}, u32[]{:S(2)}) collective-permute-start(bf16[256,256]{1,0:T(8,128)(2,1)S(1)} %fusion.4.refs_0_), channel_id=1, source_target_pairs={{0,12},{2,14},{4,0},{6,2},{8,4},{10,6},{12,8},{14,10},{1,13},{3,15... | collective-permute-start | bytes 393224 | tf_op jit(solution)/shard_map/ppermute | solution.py:43
  191.8 14.2 %collective-permute-start.21 = (bf16[256,256]{1,0:T(8,128)(2,1)S(1)}, bf16[256,256]{1,0:T(8,128)(2,1)S(1)}, u32[]{:S(2)}, u32[]{:S(2)}) collective-permute-start(bf16[256,256]{1,0:T(8,128)(2,1)S(1)} %collective-permute-done.19.refs_1_), channel_id=1, source_target_pairs={{0,12},{2,14},{4,0},{6,2},{8,4},{10,6},{12,8},{14,10},{1,13},{3,15... | collective-permute-start | bytes 393224 | tf_op jit(solution)/shard_map/ppermute | solution.py:43
  193.7 12.3 %collective-permute-start.26 = (bf16[256,256]{1,0:T(8,128)(2,1)S(1)}, bf16[256,256]{1,0:T(8,128)(2,1)S(1)}, u32[]{:S(2)}, u32[]{:S(2)}) collective-permute-start(bf16[256,256]{1,0:T(8,128)(2,1)S(1)} %collective-permute-done.25.refs_8_), channel_id=1, source_target_pairs={{0,4},{2,6},{4,8},{6,10},{8,12},{10,14},{12,0},{14,2},{1,5},{3,7},... | collective-permute-start | bytes 393224 | tf_op jit(solution)/shard_map/ppermute | solution.py:43
  197.6 7.8 %collective-permute-start.23 = (bf16[128,256]{1,0:T(8,128)(2,1)S(1)}, bf16[128,256]{1,0:T(8,128)(2,1)S(1)}, u32[]{:S(2)}, u32[]{:S(2)}) collective-permute-start(bf16[128,256]{1,0:T(8,128)(2,1)S(1)} %slice.70), channel_id=1, source_target_pairs={{0,4},{2,6},{4,8},{6,10},{8,12},{10,14},{12,0},{14,2},{1,5},{3,7},... | collective-permute-start | bytes 196616 | tf_op jit(solution)/shard_map/ppermute | solution.py:43
  198.7 7.3 %collective-permute-start.24 = (bf16[128,256]{1,0:T(8,128)(2,1)S(1)}, bf16[128,256]{1,0:T(8,128)(2,1)S(1)}, u32[]{:S(2)}, u32[]{:S(2)}) collective-permute-start(bf16[128,256]{1,0:T(8,128)(2,1)S(1)} %slice.71), channel_id=1, source_target_pairs={{0,12},{2,14},{4,0},{6,2},{8,4},{10,6},{12,8},{14,10},{1,13},{3,15... | collective-permute-start | bytes 196616 | tf_op jit(solution)/shard_map/ppermute | solution.py:43
  240.3 16.3 %collective-permute-start.27 = (bf16[8,256,256]{2,1,0:T(8,128)(2,1)}, bf16[8,256,256]{2,1,0:T(8,128)(2,1)S(1)}, u32[]{:S(2)}, u32[]{:S(2)}) collective-permute-start(bf16[8,256,256]{2,1,0:T(8,128)(2,1)} %stack.10.r_1_), channel_id=1, source_target_pairs={{0,1},{1,0},{2,3},{3,2},{4,5},{5,4},{6,7},{7,6},{8,9},{9,8},{10,11... | collective-permute-start | bytes 3145736 | tf_op jit(solution)/shard_map/ppermute | solution.py:47
  260.4 14.1 %all-to-all-start.4 = ((f32[16,1,512]{2,1,0:T(1,128)}), f32[16,1,512]{2,1,0:T(1,128)S(1)}, u32[]{:S(2)}, u32[]{:S(2)}) async-start(f32[16,1,512]{2,1,0:T(1,128)} %broadcast_in_dim.20), calls=%async_computation.4 | async-start | bytes 65536 | tf_op jit(solution)/shard_map/all_to_all | solution.py:16
  274.5 20.2 %all-to-all-start.3 = ((bf16[16,128,256]{2,1,0:T(8,128)(2,1)}), bf16[16,128,256]{2,1,0:T(8,128)(2,1)S(1)}, u32[]{:S(2)}, u32[]{:S(2)}) async-start(bf16[16,128,256]{2,1,0:T(8,128)(2,1)} %outer.1), calls=%async_computation.3 | async-start | bytes 2097152 | tf_op jit(solution)/shard_map/all_to_all | solution.py:630
  278.7 16.8 %collective-permute-start.28 = (f32[32,128]{1,0:T(8,128)S(1)}, f32[32,128]{1,0:T(8,128)S(1)}, u32[]{:S(2)}, u32[]{:S(2)}) collective-permute-start(f32[32,128]{1,0:T(8,128)S(1)} %slice.72), channel_id=1, source_target_pairs={{16,0},{32,16},{48,32},{64,48},{80,64},{96,80},{112,96},{128,112},... | collective-permute-start | bytes 49160 | tf_op jit(solution)/shard_map/ppermute | solution.py:628
  (50 other events, 758.7 us)
where the time goes:
time: 299 us; the launch traced here: 298 us
  waiting for transfers between devices  90.4 us (30%)
  Pallas kernels  79 us (26%)
  starting transfers between devices  75.2 us (25%)
  local copies, waits for them, and re-layouts  25.5 us (9%)
  blocking collectives  22.8 us (8%)
  other arithmetic  3.5 us (1%)
    ppermute x8, waiting for transfers between devices, right(): return lax.ppermute(x, 'z', [(i, (i + 1) % n) for i in range(n)])  58 us
    pallas_call x1, Pallas kernels, per_device(): pl.pallas_call(stack_body, out_shape=jax.ShapeDtypeStruct((n_z, tok_rows,...  32.9 us
    all_to_all x1, blocking collectives, per_device(): lax.all_to_all(sent.reshape(2 * experts, capacity, width_part), ('sp', 'c...  22.8 us
    ppermute x8, starting transfers between devices, left(): return lax.ppermute(x, 'z', [(i, (i - 1) % n) for i in range(n)])  21.9 us
    unnamed x105, local copies, waits for them, and re-layouts  19.6 us
    pallas_call x2, Pallas kernels, grads(): pl.pallas_call(lambda *r: grads_body(*r, n=n, add=add), out_shape=out_sha...  16.5 us
    all_to_all x1, waiting for transfers between devices, per_device(): lax.all_to_all(out_parts, 'sp', 0, 0, tiled=True).astype(F4)  14.7 us
    all_to_all x1, starting transfers between devices, per_device(): lax.all_to_all(sent_back.reshape(2 * n_sp, half_cap, width_part + 128), (...  14.4 us
  transfers between devices with their start and end apart: 33, of which 14 were waited for; matrix products, arithmetic and copies ran while one was open for 3% of the time, Pallas kernels for 23%

commit v1 on v0

--- a/solution.py
+++ b/solution.py
@@ -62,7 +62,14 @@
 BIG = pltpu.CompilerParams(vmem_limit_bytes=40 * 2**20)
 
 
-def scatter_body(routes, weights, upstream, stream, picker, sent, *, experts, capacity):
+def scatter_body(
+    routes_h, weights_h, upstream_h, stream_h, picker, sent, *scratch, experts, capacity
+):
+    routes, weights, upstream, stream, sems = scratch
+    load_all(
+        [(routes_h, routes), (weights_h, weights), (upstream_h, upstream), (stream_h, stream)],
+        sems,
+    )
     toks = upstream.shape[0]
     slots = experts * capacity
     half = capacity // 2
@@ -108,9 +115,11 @@
     lax.fori_loop(0, 2 * slots // step, rows_at, 0)
 
 
-def offset_of(k, n):
-    h = n // 2
-    return jnp.where(k < h, jnp.where(k == 0, 0, n - k), jnp.where(k == n - 1, h, k - h + 1))
+def offset_of(k, offsets, n):
+    off = jnp.int32(0)
+    for i, value in enumerate(offsets):
+        off = jnp.where(k == i, value % n, off)
+    return off
 
 
 def load_all(pairs, sems):
@@ -121,27 +130,41 @@
         copy.wait()
 
 
-def project_body(z, *refs, n):
-    blocks, refs = refs[: n - 1], refs[n - 1 :]
-    guo, gux, dno, dnx, gains, inv, own, oth, back, xs = refs[:10]
-    buf, guo_v, gux_v, dno_v, dnx_v, sems = refs[10:]
+def project_body(z, *refs, offsets, n, more):
+    m = len(offsets)
+    blocks, refs = refs[:m], refs[m:]
+    guo, gux, dno, dnx, gains, inv = refs[:6]
+    refs = refs[6:]
+    if more:
+        starts, refs = refs[:3], refs[3:]
+    sums, xs = refs[:3], refs[3]
+    own, oth, back = sums
+    buf, xs_v, guo_v, gux_v, dno_v, dnx_v, sems = refs[4:]
     rows, width = own.shape[0], buf.shape[2]
     hid = dno.shape[0]
-    load_all(
-        [(guo, guo_v), (gux, gux_v), (dno, dno_v), (dnx, dnx_v)]
-        + [(blocks[i], buf.at[i]) for i in range(n - 1)],
-        sems,
-    )
-    own[...] = jnp.zeros(own.shape, F4)
-    oth[...] = jnp.zeros(oth.shape, F4)
-    back[...] = jnp.zeros(back.shape, F4)
+    pairs = [(blocks[i], buf.at[i]) for i in range(m)]
+    if more:
+        for i, off in enumerate(offsets):
+            at = pl.multiple_of(lax.rem(z[0] + off % n, n) * width, width)
+            mine = pl.ds(i * width, width)
+            pairs += [
+                (guo.at[pl.ds(at, width), :], guo_v.at[mine, :]),
+                (gux.at[pl.ds(at, width), :], gux_v.at[mine, :]),
+                (dno.at[:, pl.ds(at, width)], dno_v.at[:, mine]),
+                (dnx.at[:, pl.ds(at, width)], dnx_v.at[:, mine]),
+            ]
+    else:
+        pairs += [(guo, guo_v), (gux, gux_v), (dno, dno_v), (dnx, dnx_v)]
+    load_all(pairs, sems)
+    for i, total in enumerate(sums):
+        total[...] = starts[i][...] if more else jnp.zeros(total.shape, F4)
 
     def step(k, carry):
-        chip = lax.rem(z[0] + offset_of(k, n), n)
-        at = pl.multiple_of(chip * width, width)
+        chip = lax.rem(z[0] + offset_of(k, offsets, n), n)
+        at = pl.multiple_of((k if more else chip) * width, width)
         x = buf[k, :rows, :].astype(F4)
         x = (gains[pl.ds(chip, 1), :] * x * inv[...]).astype(BF)
-        xs[pl.ds(pl.multiple_of(k * rows, rows), rows), :] = x
+        xs_v[pl.ds(pl.multiple_of(k * rows, rows), rows), :] = x
         own[...] += dot(x, guo_v[pl.ds(at, width), :], 1, 0)
         oth[...] += dot(x, gux_v[pl.ds(at, width), :], 1, 0)
         c = buf[k, rows:, :]
@@ -149,7 +172,34 @@
         back[:, hid:] += dot(c, dnx_v[:, pl.ds(at, width)], 1, 1)
         return carry
 
-    lax.fori_loop(0, n - 1, step, 0)
+    lax.fori_loop(0, m, step, 0)
+    load_all([(xs_v, xs)], sems)
+
+
+def project(z, blocks, weights, gains, inv, offsets, n, starts):
+    rows2, wide = blocks[0].shape
+    rows, m = rows2 // 2, len(blocks)
+    hid = weights[2].shape[0]
+    more = starts is not None
+    cols = m * wide if more else n * wide
+    total = jax.ShapeDtypeStruct((rows, 2 * hid), F4)
+    return pl.pallas_call(
+        lambda *r: project_body(*r, offsets=offsets, n=n, more=more),
+        out_shape=(total, total, total, jax.ShapeDtypeStruct((m * rows, wide), BF)),
+        in_specs=[SMEM] + [ANY] * (m + 4) + [VMEM] * (5 if more else 2),
+        out_specs=(VMEM, VMEM, VMEM, ANY),
+        scratch_shapes=[
+            pltpu.VMEM((m, rows2, wide), BF),
+            pltpu.VMEM((m * rows, wide), BF),
+            pltpu.VMEM((cols, 2 * hid), BF),
+            pltpu.VMEM((cols, 2 * hid), BF),
+            pltpu.VMEM((hid, cols), BF),
+            pltpu.VMEM((hid, cols), BF),
+            pltpu.SemaphoreType.DMA((5 * m + 4,)),
+        ],
+        compiler_params=BIG,
+        name="project",
+    )(z, *blocks, *weights, gains, inv, *(starts or ()))
 
 
 def in_parts(row):
@@ -173,7 +223,10 @@
 
 
 def finish_body(z, xf, cf, guo, gux, dno, dnx, gains, inv, own, oth, back, *refs, n):
-    x4, b_own, b_oth, a_own, a_oth, along, send_r, send_l = refs[:8]
+    hbm, refs = refs[:5], refs[5:]
+    along, send_r, send_l = refs[:3]
+    held = refs[3:8]
+    x4, b_own, b_oth, a_own, a_oth = held
     guo_v, gux_v, dno_v, dnx_v, sems = refs[8:]
     rows, width = xf.shape
     hid = dno.shape[0]
@@ -208,6 +261,11 @@
         total = total + jnp.sum(
             gb.astype(F4) * gate + ub.astype(F4) * upper, axis=1, keepdims=True
         )
+    copies = [
+        pltpu.make_async_copy(a, b, sems.at[i]) for i, (a, b) in enumerate(zip(held, hbm))
+    ]
+    for copy in copies:
+        copy.start()
     row = jnp.broadcast_to(total, (rows, 128)).T[0:8, :]
     along[:, :rows] = row
     along[:, rows:] = jnp.zeros((8, width - rows), F4)
@@ -216,10 +274,27 @@
     send_r[:hr, :] = part[:hr].astype(BF)
     send_r[hr:, :] = part_rows(along[0:1, :])
     send_l[...] = part[hr:].astype(BF)
-
-
-def parts_body(b_own, b_oth, guo, gux, out):
-    out[...] = (dot(b_own[...], guo[...], 1, 1) + dot(b_oth[...], gux[...], 1, 1)).astype(BF)
+    for copy in copies:
+        copy.wait()
+
+
+def parts_body(b_own, b_oth, guo, gux, out, guo_v, gux_v, sems, *, n):
+    width = guo.shape[0] // n
+    pairs = []
+    for k in range(n):
+        at = pl.ds(k * width, width)
+        pairs.append((guo.at[at, :], guo_v.at[at, :]))
+        pairs.append((gux.at[at, :], gux_v.at[at, :]))
+    copies = [pltpu.make_async_copy(a, b, sems.at[i]) for i, (a, b) in enumerate(pairs)]
+    for copy in copies:
+        copy.start()
+    for k in range(n):
+        copies[2 * k].wait()
+        copies[2 * k + 1].wait()
+        at = pl.ds(k * width, width)
+        out[:, at] = (
+            dot(b_own[...], guo_v[at, :], 1, 1) + dot(b_oth[...], gux_v[at, :], 1, 1)
+        ).astype(BF)
 
 
 def hop_body(z, parts, along, ra, la, out_r, out_l, *, k, n, first):
@@ -269,11 +344,11 @@
         out[2 * s * step : 2 * (s + 1) * step, half:] = jnp.concatenate([e, e], axis=0).astype(BF)
 
 
-def grads_body(z, *refs, n, add):
-    xs, x4 = refs[0], refs[1]
-    blocks, cf = refs[2 : n + 1], refs[n + 1]
-    backs, act = refs[n + 2], refs[n + 3]
-    refs = refs[n + 4 :]
+def grads_body(z, *refs, n, add, offsets):
+    xs1, xs2, x4 = refs[:3]
+    blocks, cf = refs[3 : n + 2], refs[n + 2]
+    backs, act = refs[n + 3], refs[n + 4]
+    refs = refs[n + 5 :]
     if add:
         old, gate, up, down, xbuf, cbuf, sems = refs
     else:
@@ -281,8 +356,13 @@
     rows, width = x4.shape
     hid = act.shape[1]
     near = (n - 1) * rows
+    first = xs1.shape[0]
     load_all(
-        [(xs, xbuf.at[pl.ds(0, near), :]), (x4, xbuf.at[pl.ds(near, rows), :])]
+        [
+            (xs1, xbuf.at[pl.ds(0, first), :]),
+            (xs2, xbuf.at[pl.ds(first, near - first), :]),
+            (x4, xbuf.at[pl.ds(near, rows), :]),
+        ]
         + [
             (blocks[i].at[pl.ds(rows, rows), :], cbuf.at[pl.ds(i * rows, rows), :])
             for i in range(n - 1)
@@ -292,7 +372,7 @@
     )
 
     def step(k, carry):
-        at = pl.multiple_of(lax.rem(z[0] + offset_of(k, n), n) * width, width)
+        at = pl.multiple_of(lax.rem(z[0] + offset_of(k, offsets, n), n) * width, width)
         mine = pl.ds(pl.multiple_of(k * rows, rows), rows)
         pair = dot(xbuf[mine, :], backs[...], 0, 0)
         dn = dot(act[...], cbuf[mine, :], 0, 0)
@@ -315,12 +395,12 @@
     lax.fori_loop(0, n, step, 0)
 
 
-def grads(z, xs, x4, blocks, cf, backs, act, old):
+def grads(z, xs, x4, blocks, cf, backs, act, old, offsets):
     rows, width = x4.shape
     n, hid = len(blocks) + 1, act.shape[1]
     add = old is not None
     total = n * width
-    args = [z, xs, x4, *blocks, cf, backs, act] + ([old] if add else [])
+    args = [z, *xs, x4, *blocks, cf, backs, act] + ([old] if add else [])
     if add:
         out_shape = tuple(
             jax.ShapeDtypeStruct(t, F4) for t in ((total, hid), (total, hid), (hid, total))
@@ -329,14 +409,14 @@
     else:
         out_shape, out_specs = jax.ShapeDtypeStruct((3, total, hid), BF), VMEM
     return pl.pallas_call(
-        lambda *r: grads_body(*r, n=n, add=add),
+        lambda *r: grads_body(*r, n=n, add=add, offsets=offsets),
         out_shape=out_shape,
-        in_specs=[SMEM] + [ANY] * (n + 2) + [VMEM] * (3 if add else 2),
+        in_specs=[SMEM] + [ANY] * (n + 3) + [VMEM] * (3 if add else 2),
         out_specs=out_specs,
         scratch_shapes=[
             pltpu.VMEM((n * rows, width), BF),
             pltpu.VMEM((n * rows, width), BF),
-            pltpu.SemaphoreType.DMA((n + 2,)),
+            pltpu.SemaphoreType.DMA((n + 3,)),
         ],
         compiler_params=BIG,
         cost_estimate=pl.CostEstimate(
@@ -347,18 +427,13 @@
 
 
 def stack_body(*refs):
-    refs, sems = refs[:-1], refs[-1]
-    srcs, out = refs[:-1], refs[-1]
-    pairs, at = [], 0
-    flat = out.reshape(out.shape[0] * out.shape[1], out.shape[2])
-    for src in srcs:
-        pairs.append((src, flat.at[pl.ds(at, src.shape[0]), :]))
+    out, at = refs[-1], 0
+    for src in refs[:-1]:
+        out[pl.ds(at, src.shape[0]), :] = src[...]
         at += src.shape[0]
-    load_all(pairs, sems)
-
-
-def mixed_body(zc, mine, other, w_out, slope, done, out, *, n):
-    del done
+
+
+def mixed_body(zc, mine, other, w_out, slope, out, *, n):
     width = mine.shape[2]
     out[...] = jnp.zeros(out.shape, F4)
     for ref, core in ((mine, zc[1]), (other, 1 - zc[1])):
@@ -436,8 +511,15 @@
             jax.ShapeDtypeStruct((slot_count, tok_rows), BF),
             jax.ShapeDtypeStruct((2 * slot_count, width_part), BF),
         ),
-        in_specs=[VMEM] * 4,
+        in_specs=[ANY] * 4,
         out_specs=(VMEM, VMEM),
+        scratch_shapes=[
+            pltpu.VMEM((2, tok_rows), jnp.int32),
+            pltpu.VMEM((2, tok_rows), F4),
+            pltpu.VMEM(upstream.shape, BF),
+            pltpu.VMEM(stream.shape, BF),
+            pltpu.SemaphoreType.DMA((4,)),
+        ],
         compiler_params=BIG,
         name="scatter",
     )(routes.T, route_weights.T, upstream, stream)
@@ -450,11 +532,6 @@
     gu_own = jnp.concatenate([w_gate[0], w_up[0]], axis=1)
     down_own = w_down[0]
     gu_oth, down_oth = swap(gu_own), swap(down_own)
-
-    r1, l1 = right(b0), left(b0)
-    r2, l2 = right(r1), left(l1)
-    r3, l3 = right(r2), left(l2)
-    xf, cf = right(r3[:rows]), left(l3[rows:])
 
     residual = stream.astype(F4)
     conv_vals = conv_pre.astype(F4)
@@ -484,29 +561,21 @@
     inverse = lax.rsqrt(row_squares / model_width + EPSILON)[:, None]
     slot_inverse = lax.rsqrt(slot_squares / model_width + EPSILON)[:, None]
 
-    blocks = [b0, r1, r2, r3, l1, l2, l3]
     weights = (gu_own, gu_oth, down_own, down_oth)
-    own, oth, back, xs = pl.pallas_call(
-        lambda *r: project_body(*r, n=n_z),
-        out_shape=(
-            jax.ShapeDtypeStruct((rows, 2 * hid), F4),
-            jax.ShapeDtypeStruct((rows, 2 * hid), F4),
-            jax.ShapeDtypeStruct((rows, 2 * hid), F4),
-            jax.ShapeDtypeStruct(((n_z - 1) * rows, wide), BF),
-        ),
-        in_specs=[SMEM] + [ANY] * (n_z - 1 + 4) + [VMEM] * 2,
-        out_specs=(VMEM,) * 4,
-        scratch_shapes=[
-            pltpu.VMEM((n_z - 1, 2 * rows, wide), BF),
-            pltpu.VMEM(gu_own.shape, BF),
-            pltpu.VMEM(gu_own.shape, BF),
-            pltpu.VMEM(down_own.shape, BF),
-            pltpu.VMEM(down_own.shape, BF),
-            pltpu.SemaphoreType.DMA((n_z + 3,)),
-        ],
-        compiler_params=BIG,
-        name="project",
-    )(zs, *blocks, *weights, gains, slot_inverse)
+    r1, l1 = right(b0), left(b0)
+    r2, l2 = right(r1), left(l1)
+    r2, l2, gains, slot_inverse = lax.optimization_barrier((r2, l2, gains, slot_inverse))
+    r3, l3 = right(r2), left(l2)
+    offsets = (0, -1, -2, 1, 2, -3, 3, 4)
+    *sums, xs1 = project(
+        zs, [b0, r1, r2, l1, l2], weights, gains, slot_inverse, offsets[:5], n_z, None
+    )
+    r3, l3, sums, xs1 = lax.optimization_barrier((r3, l3, sums, xs1))
+    xf, cf = right(r3[:rows]), left(l3[rows:])
+    own, oth, back, xs2 = project(
+        zs, [r3, l3], weights, gains, slot_inverse, offsets[5:7], n_z, sums
+    )
+    blocks = [b0, r1, r2, l1, l2, r3, l3]
 
     x4, b_own, b_oth, a_own, a_oth, along, ra, la = pl.pallas_call(
         lambda *r: finish_body(*r, n=n_z),
@@ -521,13 +590,18 @@
             jax.ShapeDtypeStruct((rows // 2, wide), BF),
         ),
         in_specs=[SMEM] + [VMEM] * 2 + [ANY] * 4 + [VMEM] * 5,
-        out_specs=(VMEM,) * 8,
+        out_specs=(ANY,) * 5 + (VMEM,) * 3,
         scratch_shapes=[
+            pltpu.VMEM((rows, wide), BF),
+            pltpu.VMEM((rows, 2 * hid), BF),
+            pltpu.VMEM((rows, 2 * hid), BF),
+            pltpu.VMEM((rows, hid), BF),
+            pltpu.VMEM((rows, hid), BF),
             pltpu.VMEM((wide, 2 * hid), BF),
             pltpu.VMEM((wide, 2 * hid), BF),
             pltpu.VMEM((hid, wide), BF),
             pltpu.VMEM((hid, wide), BF),
-            pltpu.SemaphoreType.DMA((4,)),
+            pltpu.SemaphoreType.DMA((5,)),
         ],
         compiler_params=BIG,
         name="finish",
@@ -535,16 +609,16 @@
 
     ra, la = right(ra), left(la)
     parts = pl.pallas_call(
-        parts_body,
-        grid=(n_z,),
+        lambda *r: parts_body(*r, n=n_z),
         out_shape=jax.ShapeDtypeStruct((rows, model_width), BF),
-        in_specs=[
-            pl.BlockSpec((rows, 2 * hid), lambda i: (0, 0)),
-            pl.BlockSpec((rows, 2 * hid), lambda i: (0, 0)),
-            pl.BlockSpec((wide, 2 * hid), lambda i: (i, 0)),
-            pl.BlockSpec((wide, 2 * hid), lambda i: (i, 0)),
+        in_specs=[VMEM] * 2 + [ANY] * 2,
+        out_specs=VMEM,
+        scratch_shapes=[
+            pltpu.VMEM(gu_own.shape, BF),
+            pltpu.VMEM(gu_own.shape, BF),
+            pltpu.SemaphoreType.DMA((2 * n_z,)),
         ],
-        out_specs=pl.BlockSpec((rows, wide), lambda i: (0, i)),
+        compiler_params=BIG,
         name="parts",
     )(b_own, b_oth, gu_own, gu_oth)
     message = jax.ShapeDtypeStruct((rows + 16, wide), BF)
@@ -558,6 +632,10 @@
             name="hop",
         )(zs, parts, along, ra, la)
         ra, la = right(ra), left(la)
+        if k == 2:
+            others = grads(zs, (xs1, xs2), x4, blocks, cf, b_oth, a_oth, None, offsets)
+            ra, la, others = lax.optimization_barrier((ra, la, others))
+            others = swap(others)
     sent_back = pl.pallas_call(
         lambda *r: pack_body(*r, n_sp=n_sp),
         out_shape=jax.ShapeDtypeStruct((slot_count, width_part + 128), BF),
@@ -570,10 +648,11 @@
         sent_back.reshape(2 * n_sp, half_cap, width_part + 128), ("sp", "c"), 0, 0, tiled=True
     ).reshape(slot_count, width_part + 128)
 
-    others = grads(zs, xs, x4, blocks, cf, b_oth, a_oth, None)
-    returned, others = lax.optimization_barrier((returned, others))
     grad_gate, grad_up, grad_down = grads(
-        zs, xs, x4, blocks, cf, b_own, a_own, swap(others)
+        zs, (xs1, xs2), x4, blocks, cf, b_own, a_own, others, offsets
+    )
+    returned, grad_gate, grad_up, grad_down = lax.optimization_barrier(
+        (returned, grad_gate, grad_up, grad_down)
     )
 
     token_back = dot(picker, returned, 0, 0)
@@ -588,12 +667,12 @@
     pf, mf = hops(p2[:ht], 2), hops(m2[ht:], -2)
     mine8 = pl.pallas_call(
         stack_body,
-        out_shape=jax.ShapeDtypeStruct((n_z, tok_rows, width_part), BF),
-        in_specs=[ANY] * 9,
-        out_specs=ANY,
-        scratch_shapes=[pltpu.SemaphoreType.DMA((9,))],
+        out_shape=jax.ShapeDtypeStruct((n_z * tok_rows, width_part), BF),
+        in_specs=[VMEM] * 9,
+        out_specs=VMEM,
+        compiler_params=BIG,
         name="stack",
-    )(stream_grad, m1, m2, m3, pf, mf, p3, p2, p1)
+    )(stream_grad, m1, m2, m3, pf, mf, p3, p2, p1).reshape(n_z, tok_rows, width_part)
     other8 = swap(mine8)
 
     mean_val = (conv_total / channels)[:, None]
@@ -608,11 +687,11 @@
     norm_in = pl.pallas_call(
         lambda *r: mixed_body(*r, n=n_z),
         out_shape=jax.ShapeDtypeStruct(conv_pre.shape, F4),
-        in_specs=[SMEM] + [VMEM] * 4 + [ANY],
+        in_specs=[SMEM] + [VMEM] * 4,
         out_specs=VMEM,
         compiler_params=BIG,
         name="mixed",
-    )(zc, mine8, other8, w_out, slope, grad_gate)
+    )(zc, mine8, other8, w_out, slope)
     out_parts = pl.pallas_call(
         lambda *r: outer_body(*r, n=n_z),
         out_shape=jax.ShapeDtypeStruct((n_sp, conv_pre.shape[1], width_part), BF),
@@ -626,9 +705,7 @@
         norm_in - (norm_total / channels)[:, None] - centred * (norm_cross / channels)[:, None]
     )
     next_rim = lax.ppermute(conv_back[:32], "sp", [(i + 1, i) for i in range(n_sp - 1)])
-    grad_out = jnp.sum(
-        lax.all_to_all(out_parts, "sp", 0, 0, tiled=True).astype(F4), axis=0
-    )
+    out_blocks = lax.all_to_all(out_parts, "sp", 0, 0, tiled=True)
     value_grad, gate_grad = pl.pallas_call(
         conv_body,
         out_shape=(jax.ShapeDtypeStruct(value_in.shape, BF),) * 2,
@@ -637,6 +714,8 @@
         scratch_shapes=[pltpu.VMEM((tok_rows + 32, conv_pre.shape[1]), F4)],
         name="conv",
     )(conv_back, next_rim, conv_taps, value_in, gate_in)
+    out_blocks, value_grad = lax.optimization_barrier((out_blocks, value_grad))
+    grad_out = jnp.sum(out_blocks.astype(F4), axis=0)
     return (grad_gate[None], grad_up[None], grad_down[None], grad_out, value_grad, gate_grad)
 
 

time: 299 us -> 252 us (0.84)
  Pallas kernels: 79 us -> 45.3 us
  blocking collectives: 22.8 us -> 0 us
  local copies, waits for them, and re-layouts: 25.5 us -> 14.7 us
  waiting for transfers between devices: 90.4 us -> 101 us
  starting transfers between devices: 75.2 us -> 81 us
    pallas_call x5 -> x6, Pallas kernels: 66.5 us -> 32.1 us  [the longest x2 17.8 us: grads(): pl.pallas_call(lambda *r: grads_body(*r, n=n, add=add, offsets=offsets),...]
    ppermute x8, waiting for transfers between devices: 58 us -> 27.9 us  [right(): return lax.ppermute(x, 'z', [(i, (i + 1) % n) for i in range(n)])]
    all_to_all x1 -> x0, blocking collectives: 22.8 us -> none  [per_device(): lax.all_to_all(sent.reshape(2 * experts, capacity, width_part), ('sp', 'c...]
    ppermute x8, waiting for transfers between devices: 0.02 us -> 18.9 us  [left(): return lax.ppermute(x, 'z', [(i, (i - 1) % n) for i in range(n)])]
    all_to_all x1, waiting for transfers between devices: 0.01 us -> 15.9 us  [per_device(): lax.all_to_all(jnp.broadcast_to(vector[None, None], (n_tp, 1, vector.size...]
    ppermute x1, waiting for transfers between devices: 0.01 us -> 11.8 us  [per_device(): lax.ppermute(conv_back[:32], 'sp', [(i + 1, i) for i in range(n_sp - 1)])]
    unnamed x105 -> x67, local copies, waits for them, and re-layouts: 19.6 us -> 7.85 us
    all_to_all x1 -> x2, starting transfers between devices: 3.89 us -> 15.3 us  [the longest x1 8.63 us: per_device(): lax.all_to_all(sent.reshape(2 * experts, capacity, width_part), ('sp', 'c...]
  transfers between devices with their start and end apart: 33 -> 34, of which waited for: 14 -> 15; matrix products, arithmetic and copies ran while one was open for 3% -> 3% of each run, Pallas kernels for 23% -> 15%
where the time goes in v1:
time: 252 us; the launch traced here: 251 us
  waiting for transfers between devices  101 us (40%)
  starting transfers between devices  81 us (32%)
  Pallas kernels  45.3 us (18%)
  local copies, waits for them, and re-layouts  14.7 us (6%)
  other arithmetic  5.56 us (2%)
    ppermute x8, waiting for transfers between devices, right(): return lax.ppermute(x, 'z', [(i, (i + 1) % n) for i in range(n)])  27.9 us
    ppermute x8, starting transfers between devices, left(): return lax.ppermute(x, 'z', [(i, (i - 1) % n) for i in range(n)])  23.7 us
    ppermute x8, waiting for transfers between devices, left(): return lax.ppermute(x, 'z', [(i, (i - 1) % n) for i in range(n)])  18.9 us
    pallas_call x2, Pallas kernels, grads(): pl.pallas_call(lambda *r: grads_body(*r, n=n, add=add, offsets=offsets),...  17.8 us
    all_to_all x1, waiting for transfers between devices, per_device(): lax.all_to_all(jnp.broadcast_to(vector[None, None], (n_tp, 1, vector.size...  15.9 us
    ppermute x8, starting transfers between devices, hops(): return lax.ppermute(x, 'z', [(i, (i + n_hops) % n) for i in range(n)])  14.5 us
    all_to_all x1, waiting for transfers between devices, per_device(): lax.all_to_all(sent.reshape(2 * experts, capacity, width_part), ('sp', 'c...  12.2 us
    ppermute x1, waiting for transfers between devices, per_device(): lax.ppermute(conv_back[:32], 'sp', [(i + 1, i) for i in range(n_sp - 1)])  11.8 us
  transfers between devices with their start and end apart: 34, of which 15 were waited for; matrix products, arithmetic and copies ran while one was open for 3% of the time, Pallas kernels for 15%

profile of v1, /device:TPU:1, one launch (start us, length us, event | category | flops | bytes accessed | tf_op | source)
XLA Modules:
  0.0 250.7 jit_solution(15897689854761930499)
XLA Ops:
  3.8 2.9 %scatter.1 = (bf16[768,256]{1,0:T(8,128)(2,1)S(1)}, bf16[1536,256]{1,0:T(8,128)(2,1)}) custom-call(s32[2,256]{1,0:T(2,128)S(1)} %bitcast.34, f32[2,256]{1,0:T(2,128)S(1)} %bitcast.35, bf16[256,256]{1,0:T(8,128)(2,1)S(1)} %copy-done.4, bf16[256,256]{1,0:T(8,128)(2,1)S(1)} %copy-done.1), custom_call_target="tpu_custom_call" | custom-call | tf_op jit(solution)/shard_map/scatter/pallas_call | solution.py:508
  7.5 8.6 %all-to-all-start = ((bf16[32,48,256]{2,1,0:T(8,128)(2,1)}), bf16[32,48,256]{2,1,0:T(8,128)(2,1)}, u32[]{:S(2)}, u32[]{:S(2)}) async-start(bf16[32,48,256]{2,1,0:T(8,128)(2,1)} %bitcast.3), calls=%async_computation | async-start | bytes 1572864 | tf_op jit(solution)/shard_map/all_to_all | solution.py:526
  18.2 12.2 %all-to-all-done = bf16[32,48,256]{2,1,0:T(8,128)(2,1)} async-done(((bf16[32,48,256]{2,1,0:T(8,128)(2,1)}), bf16[32,48,256]{2,1,0:T(8,128)(2,1)}, u32[]{:S(2)}, u32[]{:S(2)}) %all-to-all-start) | async-done | bytes 786464 | tf_op jit(solution)/shard_map/all_to_all | solution.py:526
  33.2 5.6 %collective-permute-start.2 = (bf16[768,512]{1,0:T(8,128)(2,1)}, bf16[768,512]{1,0:T(8,128)(2,1)}, u32[]{:S(2)}, u32[]{:S(2)}) collective-permute-start(bf16[768,512]{1,0:T(8,128)(2,1)} %bitcast.21.r_1_.r_4_), channel_id=1, source_target_pairs={{0,14},{2,0},{4,2},{6,4},{8,6},{10,8},{12,10},{14,12},{1,15},{3,1}... | collective-permute-start | bytes 2359304 | tf_op jit(solution)/shard_map/ppermute | solution.py:38
  40.2 15.2 %collective-permute-done.2.r_4_.r_7_ = bf16[768,512]{1,0:T(8,128)(2,1)} collective-permute-done((bf16[768,512]{1,0:T(8,128)(2,1)}, bf16[768,512]{1,0:T(8,128)(2,1)}, u32[]{:S(2)}, u32[]{:S(2)}) %collective-permute-start.2) | collective-permute-done | bytes 786464 | tf_op jit(solution)/shard_map/ppermute | solution.py:38
  55.5 3.4 %collective-permute-start.3 = (bf16[768,512]{1,0:T(8,128)(2,1)}, bf16[768,512]{1,0:T(8,128)(2,1)}, u32[]{:S(2)}, u32[]{:S(2)}) collective-permute-start(bf16[768,512]{1,0:T(8,128)(2,1)} %collective-permute-done.2.r_4_.r_7_), channel_id=1, source_target_pairs={{0,14},{2,0},{4,2},{6,4},{8,6},{10,8},{12,10},{14,12},{1,15},{3,1}... | collective-permute-start | bytes 2359304 | tf_op jit(solution)/shard_map/ppermute | solution.py:38
  59.7 6.2 %all-to-all-start.1 = ((f32[16,1,1792]{2,1,0:T(1,128)}), f32[16,1,1792]{2,1,0:T(1,128)S(1)}, u32[]{:S(2)}, u32[]{:S(2)}) async-start(f32[16,1,1792]{2,1,0:T(1,128)} %broadcast_in_dim.15), calls=%async_computation.1 | async-start | bytes 229376 | tf_op jit(solution)/shard_map/all_to_all | solution.py:551
  66.1 15.9 %all-to-all-done.1 = f32[16,1,1792]{2,1,0:T(1,128)S(1)} async-done(((f32[16,1,1792]{2,1,0:T(1,128)}), f32[16,1,1792]{2,1,0:T(1,128)S(1)}, u32[]{:S(2)}, u32[]{:S(2)}) %all-to-all-start.1) | async-done | bytes 114720 | tf_op jit(solution)/shard_map/all_to_all | solution.py:551
  86.2 6.9 %project.2 = (f32[384,256]{1,0:T(8,128)S(1)}, f32[384,256]{1,0:T(8,128)S(1)}, f32[384,256]{1,0:T(8,128)S(1)}, bf16[1920,512]{1,0:T(8,128)(2,1)S(1)}) custom-call(s32[1]{0:T(128)} %bitcast.r_0_, bf16[768,512]{1,0:T(8,128)(2,1)} %bitcast.21.r_1_.r_4_, bf16[768,512]{1,0:T(8,128)(2,1)} %collective-permute-done.r_2_.r_5_, ...), custom_call_target="tpu_custom_call" | custom-call | tf_op jit(solution)/shard_map/project/pallas_call | solution.py:186
  93.0 9.5 %collective-permute-done.4.r_1_.r_9_ = bf16[768,512]{1,0:T(8,128)(2,1)} collective-permute-done((bf16[768,512]{1,0:T(8,128)(2,1)}, bf16[768,512]{1,0:T(8,128)(2,1)}, u32[]{:S(2)}, u32[]{:S(2)}) %collective-permute-start.4) | collective-permute-done | bytes 786464 | tf_op jit(solution)/shard_map/ppermute | solution.py:33
  107.0 3.1 %project.3 = (f32[384,256]{1,0:T(8,128)S(1)}, f32[384,256]{1,0:T(8,128)S(1)}, f32[384,256]{1,0:T(8,128)S(1)}, bf16[768,512]{1,0:T(8,128)(2,1)S(1)}) custom-call(s32[1]{0:T(128)} %bitcast.r_0_, bf16[768,512]{1,0:T(8,128)(2,1)} %collective-permute-done.4.r_1_.r_9_, bf16[768,512]{1,0:T(8,128)(2,1)} %collective-permute-done.5.r_2_.r_10_, ...), custom_call_target="tpu_custom_call" | custom-call | tf_op jit(solution)/shard_map/project/pallas_call | solution.py:186
  110.2 3.6 %collective-permute-done.9.r_2_.r_11_ = bf16[384,512]{1,0:T(8,128)(2,1)S(1)} collective-permute-done((bf16[384,512]{1,0:T(8,128)(2,1)S(1)}, bf16[384,512]{1,0:T(8,128)(2,1)S(1)}, u32[]{:S(2)}, u32[]{:S(2)}) %collective-permute-start.9) | collective-permute-done | bytes 393248 | tf_op jit(solution)/shard_map/ppermute | solution.py:38
  113.8 3.0 %collective-permute-done.8.r_1_ = bf16[384,512]{1,0:T(8,128)(2,1)S(1)} collective-permute-done((bf16[384,512]{1,0:T(8,128)(2,1)S(1)}, bf16[384,512]{1,0:T(8,128)(2,1)S(1)}, u32[]{:S(2)}, u32[]{:S(2)}) %collective-permute-start.8) | collective-permute-done | bytes 393248 | tf_op jit(solution)/shard_map/ppermute | solution.py:33
  116.8 3.2 %finish.1 = (bf16[384,512]{1,0:T(8,128)(2,1)S(1)}, bf16[384,256]{1,0:T(8,128)(2,1)S(1)}, bf16[384,256]{1,0:T(8,128)(2,1)S(1)}, bf16[384,128]{1,0:T(8,128)(2,1)S(...) custom-call(s32[1]{0:T(128)} %bitcast.r_0_, ...), custom_call_target="tpu_custom_call" | custom-call | tf_op jit(solution)/shard_map/finish/pallas_call | solution.py:580
  120.1 2.7 %collective-permute-start.11 = (bf16[192,512]{1,0:T(8,128)(2,1)S(1)}, bf16[192,512]{1,0:T(8,128)(2,1)S(1)}, u32[]{:S(2)}, u32[]{:S(2)}) collective-permute-start(bf16[192,512]{1,0:T(8,128)(2,1)S(1)} %get-tuple-element.75), channel_id=1, source_target_pairs={{0,14},{2,0},{4,2},{6,4},{8,6},{10,8},{12,10},{14,12},{1,15},{3,1}... | collective-permute-start | bytes 589832 | tf_op jit(solution)/shard_map/ppermute | solution.py:38
  122.7 4.3 %parts.1.r_1_ = bf16[384,4096]{1,0:T(8,128)(2,1)S(1)} custom-call(bf16[384,256]{1,0:T(8,128)(2,1)S(1)} %get-tuple-element.71.r_0_.r_12_, bf16[384,256]{1,0:T(8,128)(2,1)S(1)} %get-tuple-element.72.r_1_.r_12_, bf16[4096,256]{1,0:T(8,128)(2,1)S(1)} %pad_maximum_fusion.r_6_.r_3_.r_2_, bf16[4096,256]{1,0:T(8,128)(2,1)} %collective-permute-done.6.r_7_.r_4_.r_3_), custom_call_target="tpu_custom_call" | custom-call | tf_op jit(solution)/shard_map/parts/pallas_call | solution.py:611
  130.0 6.0 %collective-permute-done.12.r_3_ = bf16[400,512]{1,0:T(8,128)(2,1)S(1)} collective-permute-done((bf16[400,512]{1,0:T(8,128)(2,1)S(1)}, bf16[400,512]{1,0:T(8,128)(2,1)S(1)}, u32[]{:S(2)}, u32[]{:S(2)}) %collective-permute-start.12) | collective-permute-done | bytes 409632 | tf_op jit(solution)/shard_map/ppermute | solution.py:33
  139.0 7.4 %grads_other.1 = bf16[3,4096,128]{2,1,0:T(8,128)(2,1)} custom-call(s32[1]{0:T(128)} %bitcast.r_0_, bf16[1920,512]{1,0:T(8,128)(2,1)S(1)} %get-tuple-element.80.r_1_, bf16[768,512]{1,0:T(8,128)(2,1)S(1)} %get-tuple-element.81.r_2_, bf16[384,512]{1,0:T(8,128)(2,1)S(1)} %get-tuple-element.82.r_3_, bf16[768,512]{1,0:T(8,128)(2,1)} %bitcast.21.r_1_.r_4_, ...), custom_call_target="tpu_custom_call" | custom-call | flops 4831838208 | bytes 16777216 | tf_op jit(solution)/shard_map/grads_other/pallas_call | solution.py:411
  146.4 5.1 %collective-permute-start.18 = (bf16[3,4096,128]{2,1,0:T(8,128)(2,1)}, bf16[3,4096,128]{2,1,0:T(8,128)(2,1)}, u32[]{:S(2)}, u32[]{:S(2)}) collective-permute-start(bf16[3,4096,128]{2,1,0:T(8,128)(2,1)} %grads_other.1), channel_id=1, source_target_pairs={{0,1},{1,0},{2,3},{3,2},{4,5},{5,4},{6,7},{7,6},{8,9},{9,8},{10,11... | collective-permute-start | bytes 9437192 | tf_op jit(solution)/shard_map/ppermute | solution.py:47
  151.9 2.7 %collective-permute-start.17 = (bf16[400,512]{1,0:T(8,128)(2,1)S(1)}, bf16[400,512]{1,0:T(8,128)(2,1)S(1)}, u32[]{:S(2)}, u32[]{:S(2)}) collective-permute-start(bf16[400,512]{1,0:T(8,128)(2,1)S(1)} %get-tuple-element.87), channel_id=1, source_target_pairs={{0,14},{2,0},{4,2},{6,4},{8,6},{10,8},{12,10},{14,12},{1,15},{3,1}... | collective-permute-start | bytes 1228808 | tf_op jit(solution)/shard_map/ppermute | solution.py:38
  154.6 9.4 %collective-permute-done.16.r_3_ = bf16[400,512]{1,0:T(8,128)(2,1)S(1)} collective-permute-done((bf16[400,512]{1,0:T(8,128)(2,1)S(1)}, bf16[400,512]{1,0:T(8,128)(2,1)S(1)}, u32[]{:S(2)}, u32[]{:S(2)}) %collective-permute-start.16) | collective-permute-done | bytes 409632 | tf_op jit(solution)/shard_map/ppermute | solution.py:33
  165.3 5.8 %all-to-all-start.2 = ((bf16[32,24,384]{2,1,0:T(8,128)(2,1)}), bf16[32,24,384]{2,1,0:T(8,128)(2,1)}, u32[]{:S(2)}, u32[]{:S(2)}) async-start(bf16[32,24,384]{2,1,0:T(8,128)(2,1)} %bitcast.10), calls=%async_computation.2 | async-start | bytes 1179648 | tf_op jit(solution)/shard_map/all_to_all | solution.py:647
  173.3 10.4 %grads_own.1 = (f32[4096,128]{1,0:T(8,128)}, f32[4096,128]{1,0:T(8,128)}, f32[128,4096]{1,0:T(8,128)}) custom-call(s32[1]{0:T(128)} %bitcast.r_0_, bf16[1920,512]{1,0:T(8,128)(2,1)S(1)} %copy-done.15, bf16[768,512]{1,0:T(8,128)(2,1)S(1)} %copy-done.17, bf16[384,512]{1,0:T(8,128)(2,1)S(1)} %copy-done.19, bf16[768,512]{1,0:T(8,128)(2,1)} %bitcast.21.r_1_.r_4_, ...), custom_call_target="tpu_custom_call" | custom-call | flops 4831838208 | bytes 16777216 | tf_op jit(solution)/shard_map/grads_own/pallas_call | solution.py:411
  186.5 2.8 %collective-permute-start.19 = (bf16[256,256]{1,0:T(8,128)(2,1)S(1)}, bf16[256,256]{1,0:T(8,128)(2,1)S(1)}, u32[]{:S(2)}, u32[]{:S(2)}) collective-permute-start(bf16[256,256]{1,0:T(8,128)(2,1)S(1)} %fusion.4.refs_0_), channel_id=1, source_target_pairs={{0,14},{2,0},{4,2},{6,4},{8,6},{10,8},{12,10},{14,12},{1,15},{3,1}... | collective-permute-start | bytes 393224 | tf_op jit(solution)/shard_map/ppermute | solution.py:43
  189.7 3.2 %collective-permute-start.20 = (bf16[256,256]{1,0:T(8,128)(2,1)S(1)}, bf16[256,256]{1,0:T(8,128)(2,1)S(1)}, u32[]{:S(2)}, u32[]{:S(2)}) collective-permute-start(bf16[256,256]{1,0:T(8,128)(2,1)S(1)} %fusion.4.refs_0_), channel_id=1, source_target_pairs={{0,12},{2,14},{4,0},{6,2},{8,4},{10,6},{12,8},{14,10},{1,13},{3,15... | collective-permute-start | bytes 393224 | tf_op jit(solution)/shard_map/ppermute | solution.py:43
  192.9 3.6 %collective-permute-start.21 = (bf16[256,256]{1,0:T(8,128)(2,1)S(1)}, bf16[256,256]{1,0:T(8,128)(2,1)S(1)}, u32[]{:S(2)}, u32[]{:S(2)}) collective-permute-start(bf16[256,256]{1,0:T(8,128)(2,1)S(1)} %collective-permute-done.19.refs_1_), channel_id=1, source_target_pairs={{0,12},{2,14},{4,0},{6,2},{8,4},{10,6},{12,8},{14,10},{1,13},{3,15... | collective-permute-start | bytes 393224 | tf_op jit(solution)/shard_map/ppermute | solution.py:43
  198.9 4.5 %collective-permute-start.24 = (bf16[128,256]{1,0:T(8,128)(2,1)S(1)}, bf16[128,256]{1,0:T(8,128)(2,1)S(1)}, u32[]{:S(2)}, u32[]{:S(2)}) collective-permute-start(bf16[128,256]{1,0:T(8,128)(2,1)S(1)} %slice.69), channel_id=1, source_target_pairs={{0,12},{2,14},{4,0},{6,2},{8,4},{10,6},{12,8},{14,10},{1,13},{3,15... | collective-permute-start | bytes 196616 | tf_op jit(solution)/shard_map/ppermute | solution.py:43
  203.3 4.6 %collective-permute-done.23.refs_4_ = bf16[128,256]{1,0:T(8,128)(2,1)S(1)} collective-permute-done((bf16[128,256]{1,0:T(8,128)(2,1)S(1)}, bf16[128,256]{1,0:T(8,128)(2,1)S(1)}, u32[]{:S(2)}, u32[]{:S(2)}) %collective-permute-start.23) | collective-permute-done | bytes 65568 | tf_op jit(solution)/shard_map/ppermute | solution.py:43
  213.5 6.0 %all-to-all-start.4 = ((f32[16,1,512]{2,1,0:T(1,128)}), f32[16,1,512]{2,1,0:T(1,128)S(1)}, u32[]{:S(2)}, u32[]{:S(2)}) async-start(f32[16,1,512]{2,1,0:T(1,128)} %broadcast_in_dim.20), calls=%async_computation.4 | async-start | bytes 65536 | tf_op jit(solution)/shard_map/all_to_all | solution.py:16
  221.7 5.3 %all-to-all-done.4 = f32[16,1,512]{2,1,0:T(1,128)S(1)} async-done(((f32[16,1,512]{2,1,0:T(1,128)}), f32[16,1,512]{2,1,0:T(1,128)S(1)}, u32[]{:S(2)}, u32[]{:S(2)}) %all-to-all-start.4) | async-done | bytes 32800 | tf_op jit(solution)/shard_map/all_to_all | solution.py:16
  227.0 6.7 %all-to-all-start.3 = ((bf16[16,128,256]{2,1,0:T(8,128)(2,1)}), bf16[16,128,256]{2,1,0:T(8,128)(2,1)S(1)}, u32[]{:S(2)}, u32[]{:S(2)}) async-start(bf16[16,128,256]{2,1,0:T(8,128)(2,1)} %outer.1), calls=%async_computation.3 | async-start | bytes 2097152 | tf_op jit(solution)/shard_map/all_to_all | solution.py:708
  235.2 11.8 %collective-permute-done.28.rim = f32[32,128]{1,0:T(8,128)S(1)} collective-permute-done((f32[32,128]{1,0:T(8,128)S(1)}, f32[32,128]{1,0:T(8,128)S(1)}, u32[]{:S(2)}, u32[]{:S(2)}) %collective-permute-start.28) | collective-permute-done | bytes 16416 | tf_op jit(solution)/shard_map/ppermute | solution.py:707
  (154 shorter events, 48.0 us)
Async XLA Ops:
  7.5 22.9 %all-to-all-start = ((bf16[32,48,256]{2,1,0:T(8,128)(2,1)}), bf16[32,48,256]{2,1,0:T(8,128)(2,1)}, u32[]{:S(2)}, u32[]{:S(2)}) async-start(bf16[32,48,256]{2,1,0:T(8,128)(2,1)} %bitcast.3), calls=%async_computation | async-start | bytes 1572864 | tf_op jit(solution)/shard_map/all_to_all | solution.py:526
  17.7 68.5 %collective-permute-start.6 = (bf16[4096,256]{1,0:T(8,128)(2,1)S(1)}, bf16[4096,256]{1,0:T(8,128)(2,1)}, u32[]{:S(2)}, u32[]{:S(2)}) collective-permute-start(bf16[4096,256]{1,0:T(8,128)(2,1)S(1)} %pad_maximum_fusion.r_6_.r_3_.r_2_), channel_id=1, source_target_pairs={{0,1},{1,0},{2,3},{3,2},{4,5},{5,4},{6,7},{7,6},{8,9},{9,8},{10,11... | collective-permute-start | bytes 6291464 | tf_op jit(solution)/shard_map/ppermute | solution.py:47
  33.2 22.3 %collective-permute-start.2 = (bf16[768,512]{1,0:T(8,128)(2,1)}, bf16[768,512]{1,0:T(8,128)(2,1)}, u32[]{:S(2)}, u32[]{:S(2)}) collective-permute-start(bf16[768,512]{1,0:T(8,128)(2,1)} %bitcast.21.r_1_.r_4_), channel_id=1, source_target_pairs={{0,14},{2,0},{4,2},{6,4},{8,6},{10,8},{12,10},{14,12},{1,15},{3,1}... | collective-permute-start | bytes 2359304 | tf_op jit(solution)/shard_map/ppermute | solution.py:38
  38.8 20.1 %collective-permute-start = (bf16[768,512]{1,0:T(8,128)(2,1)}, bf16[768,512]{1,0:T(8,128)(2,1)}, u32[]{:S(2)}, u32[]{:S(2)}) collective-permute-start(bf16[768,512]{1,0:T(8,128)(2,1)} %bitcast.21.r_1_.r_4_), channel_id=1, source_target_pairs={{0,2},{2,4},{4,6},{6,8},{8,10},{10,12},{12,14},{14,0},{1,3},{3,5},... | collective-permute-start | bytes 2359304 | tf_op jit(solution)/shard_map/ppermute | solution.py:33
  55.5 27.2 %collective-permute-start.3 = (bf16[768,512]{1,0:T(8,128)(2,1)}, bf16[768,512]{1,0:T(8,128)(2,1)}, u32[]{:S(2)}, u32[]{:S(2)}) collective-permute-start(bf16[768,512]{1,0:T(8,128)(2,1)} %collective-permute-done.2.r_4_.r_7_), channel_id=1, source_target_pairs={{0,14},{2,0},{4,2},{6,4},{8,6},{10,8},{12,10},{14,12},{1,15},{3,1}... | collective-permute-start | bytes 2359304 | tf_op jit(solution)/shard_map/ppermute | solution.py:38
  58.9 23.8 %collective-permute-start.1 = (bf16[768,512]{1,0:T(8,128)(2,1)}, bf16[768,512]{1,0:T(8,128)(2,1)}, u32[]{:S(2)}, u32[]{:S(2)}) collective-permute-start(bf16[768,512]{1,0:T(8,128)(2,1)} %collective-permute-done.r_2_.r_5_), channel_id=1, source_target_pairs={{0,2},{2,4},{4,6},{6,8},{8,10},{10,12},{12,14},{14,0},{1,3},{3,5},... | collective-permute-start | bytes 2359304 | tf_op jit(solution)/shard_map/ppermute | solution.py:33
  59.7 22.2 %all-to-all-start.1 = ((f32[16,1,1792]{2,1,0:T(1,128)}), f32[16,1,1792]{2,1,0:T(1,128)S(1)}, u32[]{:S(2)}, u32[]{:S(2)}) async-start(f32[16,1,1792]{2,1,0:T(1,128)} %broadcast_in_dim.15), calls=%async_computation.1 | async-start | bytes 229376 | tf_op jit(solution)/shard_map/all_to_all | solution.py:551
  65.9 20.2 %collective-permute-start.7 = (bf16[128,4096]{1,0:T(8,128)(2,1)S(1)}, bf16[128,4096]{1,0:T(8,128)(2,1)}, u32[]{:S(2)}, u32[]{:S(2)}) collective-permute-start(bf16[128,4096]{1,0:T(8,128)(2,1)S(1)} %bitcast.30), channel_id=1, source_target_pairs={{0,1},{1,0},{2,3},{3,2},{4,5},{5,4},{6,7},{7,6},{8,9},{9,8},{10,11... | collective-permute-start | bytes 3145736 | tf_op jit(solution)/shard_map/ppermute | solution.py:47
  82.6 19.9 %collective-permute-start.4 = (bf16[768,512]{1,0:T(8,128)(2,1)}, bf16[768,512]{1,0:T(8,128)(2,1)}, u32[]{:S(2)}, u32[]{:S(2)}) collective-permute-start(bf16[768,512]{1,0:T(8,128)(2,1)} %collective-permute-done.1.r_3_.r_6_), channel_id=1, source_target_pairs={{0,2},{2,4},{4,6},{6,8},{8,10},{10,12},{12,14},{14,0},{1,3},{3,5},... | collective-permute-start | bytes 2359304 | tf_op jit(solution)/shard_map/ppermute | solution.py:33
  83.8 18.7 %collective-permute-start.5 = (bf16[768,512]{1,0:T(8,128)(2,1)}, bf16[768,512]{1,0:T(8,128)(2,1)}, u32[]{:S(2)}, u32[]{:S(2)}) collective-permute-start(bf16[768,512]{1,0:T(8,128)(2,1)} %collective-permute-done.3.r_5_.r_8_), channel_id=1, source_target_pairs={{0,14},{2,0},{4,2},{6,4},{8,6},{10,8},{12,10},{14,12},{1,15},{3,1}... | collective-permute-start | bytes 2359304 | tf_op jit(solution)/shard_map/ppermute | solution.py:38
  104.6 9.2 %collective-permute-start.9 = (bf16[384,512]{1,0:T(8,128)(2,1)S(1)}, bf16[384,512]{1,0:T(8,128)(2,1)S(1)}, u32[]{:S(2)}, u32[]{:S(2)}) collective-permute-start(bf16[384,512]{1,0:T(8,128)(2,1)S(1)} %slice.53), channel_id=1, source_target_pairs={{0,14},{2,0},{4,2},{6,4},{8,6},{10,8},{12,10},{14,12},{1,15},{3,1}... | collective-permute-start | bytes 1179656 | tf_op jit(solution)/shard_map/ppermute | solution.py:38
  107.0 9.7 %collective-permute-start.8 = (bf16[384,512]{1,0:T(8,128)(2,1)S(1)}, bf16[384,512]{1,0:T(8,128)(2,1)S(1)}, u32[]{:S(2)}, u32[]{:S(2)}) collective-permute-start(bf16[384,512]{1,0:T(8,128)(2,1)S(1)} %slice.52), channel_id=1, source_target_pairs={{0,2},{2,4},{4,6},{6,8},{8,10},{10,12},{12,14},{14,0},{1,3},{3,5},... | collective-permute-start | bytes 1179656 | tf_op jit(solution)/shard_map/ppermute | solution.py:33
  120.0 7.1 %collective-permute-start.10 = (bf16[208,512]{1,0:T(8,128)(2,1)S(1)}, bf16[208,512]{1,0:T(8,128)(2,1)S(1)}, u32[]{:S(2)}, u32[]{:S(2)}) collective-permute-start(bf16[208,512]{1,0:T(8,128)(2,1)S(1)} %get-tuple-element.74), channel_id=1, source_target_pairs={{0,2},{2,4},{4,6},{6,8},{8,10},{10,12},{12,14},{14,0},{1,3},{3,5},... | collective-permute-start | bytes 638984 | tf_op jit(solution)/shard_map/ppermute | solution.py:33
  120.1 7.0 %collective-permute-start.11 = (bf16[192,512]{1,0:T(8,128)(2,1)S(1)}, bf16[192,512]{1,0:T(8,128)(2,1)S(1)}, u32[]{:S(2)}, u32[]{:S(2)}) collective-permute-start(bf16[192,512]{1,0:T(8,128)(2,1)S(1)} %get-tuple-element.75), channel_id=1, source_target_pairs={{0,14},{2,0},{4,2},{6,4},{8,6},{10,8},{12,10},{14,12},{1,15},{3,1}... | collective-permute-start | bytes 589832 | tf_op jit(solution)/shard_map/ppermute | solution.py:38
  127.3 8.7 %collective-permute-start.12 = (bf16[400,512]{1,0:T(8,128)(2,1)S(1)}, bf16[400,512]{1,0:T(8,128)(2,1)S(1)}, u32[]{:S(2)}, u32[]{:S(2)}) collective-permute-start(bf16[400,512]{1,0:T(8,128)(2,1)S(1)} %get-tuple-element.76), channel_id=1, source_target_pairs={{0,2},{2,4},{4,6},{6,8},{8,10},{10,12},{12,14},{14,0},{1,3},{3,5},... | collective-permute-start | bytes 1228808 | tf_op jit(solution)/shard_map/ppermute | solution.py:33
  127.4 8.6 %collective-permute-start.13 = (bf16[400,512]{1,0:T(8,128)(2,1)S(1)}, bf16[400,512]{1,0:T(8,128)(2,1)S(1)}, u32[]{:S(2)}, u32[]{:S(2)}) collective-permute-start(bf16[400,512]{1,0:T(8,128)(2,1)S(1)} %get-tuple-element.77), channel_id=1, source_target_pairs={{0,14},{2,0},{4,2},{6,4},{8,6},{10,8},{12,10},{14,12},{1,15},{3,1}... | collective-permute-start | bytes 1228808 | tf_op jit(solution)/shard_map/ppermute | solution.py:38
  136.3 10.2 %collective-permute-start.14 = (bf16[400,512]{1,0:T(8,128)(2,1)S(1)}, bf16[400,512]{1,0:T(8,128)(2,1)S(1)}, u32[]{:S(2)}, u32[]{:S(2)}) collective-permute-start(bf16[400,512]{1,0:T(8,128)(2,1)S(1)} %get-tuple-element.78), channel_id=1, source_target_pairs={{0,2},{2,4},{4,6},{6,8},{8,10},{10,12},{12,14},{14,0},{1,3},{3,5},... | collective-permute-start | bytes 1228808 | tf_op jit(solution)/shard_map/ppermute | solution.py:33
  136.3 10.1 %collective-permute-start.15 = (bf16[400,512]{1,0:T(8,128)(2,1)S(1)}, bf16[400,512]{1,0:T(8,128)(2,1)S(1)}, u32[]{:S(2)}, u32[]{:S(2)}) collective-permute-start(bf16[400,512]{1,0:T(8,128)(2,1)S(1)} %get-tuple-element.79), channel_id=1, source_target_pairs={{0,14},{2,0},{4,2},{6,4},{8,6},{10,8},{12,10},{14,12},{1,15},{3,1}... | collective-permute-start | bytes 1228808 | tf_op jit(solution)/shard_map/ppermute | solution.py:38
  146.4 24.7 %collective-permute-start.18 = (bf16[3,4096,128]{2,1,0:T(8,128)(2,1)}, bf16[3,4096,128]{2,1,0:T(8,128)(2,1)}, u32[]{:S(2)}, u32[]{:S(2)}) collective-permute-start(bf16[3,4096,128]{2,1,0:T(8,128)(2,1)} %grads_other.1), channel_id=1, source_target_pairs={{0,1},{1,0},{2,3},{3,2},{4,5},{5,4},{6,7},{7,6},{8,9},{9,8},{10,11... | collective-permute-start | bytes 9437192 | tf_op jit(solution)/shard_map/ppermute | solution.py:47
  151.8 12.3 %collective-permute-start.16 = (bf16[400,512]{1,0:T(8,128)(2,1)S(1)}, bf16[400,512]{1,0:T(8,128)(2,1)S(1)}, u32[]{:S(2)}, u32[]{:S(2)}) collective-permute-start(bf16[400,512]{1,0:T(8,128)(2,1)S(1)} %get-tuple-element.86), channel_id=1, source_target_pairs={{0,2},{2,4},{4,6},{6,8},{8,10},{10,12},{12,14},{14,0},{1,3},{3,5},... | collective-permute-start | bytes 1228808 | tf_op jit(solution)/shard_map/ppermute | solution.py:33
  151.9 12.2 %collective-permute-start.17 = (bf16[400,512]{1,0:T(8,128)(2,1)S(1)}, bf16[400,512]{1,0:T(8,128)(2,1)S(1)}, u32[]{:S(2)}, u32[]{:S(2)}) collective-permute-start(bf16[400,512]{1,0:T(8,128)(2,1)S(1)} %get-tuple-element.87), channel_id=1, source_target_pairs={{0,14},{2,0},{4,2},{6,4},{8,6},{10,8},{12,10},{14,12},{1,15},{3,1}... | collective-permute-start | bytes 1228808 | tf_op jit(solution)/shard_map/ppermute | solution.py:38
  165.3 18.4 %all-to-all-start.2 = ((bf16[32,24,384]{2,1,0:T(8,128)(2,1)}), bf16[32,24,384]{2,1,0:T(8,128)(2,1)}, u32[]{:S(2)}, u32[]{:S(2)}) async-start(bf16[32,24,384]{2,1,0:T(8,128)(2,1)} %bitcast.10), calls=%async_computation.2 | async-start | bytes 1179648 | tf_op jit(solution)/shard_map/all_to_all | solution.py:647
  186.4 6.5 %collective-permute-start.25 = (bf16[256,256]{1,0:T(8,128)(2,1)S(1)}, bf16[256,256]{1,0:T(8,128)(2,1)S(1)}, u32[]{:S(2)}, u32[]{:S(2)}) collective-permute-start(bf16[256,256]{1,0:T(8,128)(2,1)S(1)} %fusion.4.refs_0_), channel_id=1, source_target_pairs={{0,2},{2,4},{4,6},{6,8},{8,10},{10,12},{12,14},{14,0},{1,3},{3,5},... | collective-permute-start | bytes 393224 | tf_op jit(solution)/shard_map/ppermute | solution.py:43
  189.3 9.0 %collective-permute-start.22 = (bf16[256,256]{1,0:T(8,128)(2,1)S(1)}, bf16[256,256]{1,0:T(8,128)(2,1)S(1)}, u32[]{:S(2)}, u32[]{:S(2)}) collective-permute-start(bf16[256,256]{1,0:T(8,128)(2,1)S(1)} %fusion.4.refs_0_), channel_id=1, source_target_pairs={{0,4},{2,6},{4,8},{6,10},{8,12},{10,14},{12,0},{14,2},{1,5},{3,7},... | collective-permute-start | bytes 393224 | tf_op jit(solution)/shard_map/ppermute | solution.py:43
  189.7 9.2 %collective-permute-start.20 = (bf16[256,256]{1,0:T(8,128)(2,1)S(1)}, bf16[256,256]{1,0:T(8,128)(2,1)S(1)}, u32[]{:S(2)}, u32[]{:S(2)}) collective-permute-start(bf16[256,256]{1,0:T(8,128)(2,1)S(1)} %fusion.4.refs_0_), channel_id=1, source_target_pairs={{0,12},{2,14},{4,0},{6,2},{8,4},{10,6},{12,8},{14,10},{1,13},{3,15... | collective-permute-start | bytes 393224 | tf_op jit(solution)/shard_map/ppermute | solution.py:43
  192.9 15.0 %collective-permute-start.26 = (bf16[256,256]{1,0:T(8,128)(2,1)S(1)}, bf16[256,256]{1,0:T(8,128)(2,1)S(1)}, u32[]{:S(2)}, u32[]{:S(2)}) collective-permute-start(bf16[256,256]{1,0:T(8,128)(2,1)S(1)} %collective-permute-done.25.refs_8_), channel_id=1, source_target_pairs={{0,4},{2,6},{4,8},{6,10},{8,12},{10,14},{12,0},{14,2},{1,5},{3,7},... | collective-permute-start | bytes 393224 | tf_op jit(solution)/shard_map/ppermute | solution.py:43
  192.9 15.0 %collective-permute-start.21 = (bf16[256,256]{1,0:T(8,128)(2,1)S(1)}, bf16[256,256]{1,0:T(8,128)(2,1)S(1)}, u32[]{:S(2)}, u32[]{:S(2)}) collective-permute-start(bf16[256,256]{1,0:T(8,128)(2,1)S(1)} %collective-permute-done.19.refs_1_), channel_id=1, source_target_pairs={{0,12},{2,14},{4,0},{6,2},{8,4},{10,6},{12,8},{14,10},{1,13},{3,15... | collective-permute-start | bytes 393224 | tf_op jit(solution)/shard_map/ppermute | solution.py:43
  198.3 9.6 %collective-permute-start.23 = (bf16[128,256]{1,0:T(8,128)(2,1)S(1)}, bf16[128,256]{1,0:T(8,128)(2,1)S(1)}, u32[]{:S(2)}, u32[]{:S(2)}) collective-permute-start(bf16[128,256]{1,0:T(8,128)(2,1)S(1)} %slice.68), channel_id=1, source_target_pairs={{0,4},{2,6},{4,8},{6,10},{8,12},{10,14},{12,0},{14,2},{1,5},{3,7},... | collective-permute-start | bytes 196616 | tf_op jit(solution)/shard_map/ppermute | solution.py:43
  198.9 9.1 %collective-permute-start.24 = (bf16[128,256]{1,0:T(8,128)(2,1)S(1)}, bf16[128,256]{1,0:T(8,128)(2,1)S(1)}, u32[]{:S(2)}, u32[]{:S(2)}) collective-permute-start(bf16[128,256]{1,0:T(8,128)(2,1)S(1)} %slice.69), channel_id=1, source_target_pairs={{0,12},{2,14},{4,0},{6,2},{8,4},{10,6},{12,8},{14,10},{1,13},{3,15... | collective-permute-start | bytes 196616 | tf_op jit(solution)/shard_map/ppermute | solution.py:43
  213.5 13.4 %all-to-all-start.4 = ((f32[16,1,512]{2,1,0:T(1,128)}), f32[16,1,512]{2,1,0:T(1,128)S(1)}, u32[]{:S(2)}, u32[]{:S(2)}) async-start(f32[16,1,512]{2,1,0:T(1,128)} %broadcast_in_dim.20), calls=%async_computation.4 | async-start | bytes 65536 | tf_op jit(solution)/shard_map/all_to_all | solution.py:16
  227.0 23.0 %all-to-all-start.3 = ((bf16[16,128,256]{2,1,0:T(8,128)(2,1)}), bf16[16,128,256]{2,1,0:T(8,128)(2,1)S(1)}, u32[]{:S(2)}, u32[]{:S(2)}) async-start(bf16[16,128,256]{2,1,0:T(8,128)(2,1)} %outer.1), calls=%async_computation.3 | async-start | bytes 2097152 | tf_op jit(solution)/shard_map/all_to_all | solution.py:708
  233.9 13.1 %collective-permute-start.28 = (f32[32,128]{1,0:T(8,128)S(1)}, f32[32,128]{1,0:T(8,128)S(1)}, u32[]{:S(2)}, u32[]{:S(2)}) collective-permute-start(f32[32,128]{1,0:T(8,128)S(1)} %slice.70), channel_id=1, source_target_pairs={{16,0},{32,16},{48,32},{64,48},{80,64},{96,80},{112,96},{128,112},... | collective-permute-start | bytes 49160 | tf_op jit(solution)/shard_map/ppermute | solution.py:707
  (32 other events, 457.8 us)
